TPU v7x, 32 devices: a whole 2x2x4 slice. The times are simulated.
32 devices in a mesh: ep: 8 (over z, y), tp: 4 (over x, core).
Axes of the slice: x: 2, y: 2, z: 4, core: 2. Of those that a mesh axis runs over, the one named last changes fastest.
Arguments:
- query: bfloat16 [1024, 1536], P('ep', 'tp'), may hold values from -136 to 136
- latent: bfloat16 [1024, 512], P(('ep', 'tp')), may hold values from -6 to 6
- rope_key: bfloat16 [1024, 32], P(('ep', 'tp')), may hold values from -6 to 6
- latent_gain: float32 [512], replicated, may hold values from 0.1 to 1.9
- key_up: bfloat16 [512, 1024], P(None, 'tp'), may hold values from -0.25 to 0.25
- value_up: bfloat16 [512, 1024], P(None, 'tp'), may hold values from -2 to 2
- out_proj: bfloat16 [1024, 2048], replicated, may hold values from -0.1875 to 0.1875
- tokens: bfloat16 [2048, 2048], P(('ep', 'tp')), may hold values from -6 to 6
- moe_gain: float32 [2048], replicated, may hold values from 0.1 to 1.9
- routes: int32 [2048, 2], P(('ep', 'tp')), may hold values from 0 to 7, all different within a row; in each aligned block of 64 rows (0 to 63, 64 to 127, ...) at most 32 rows name the same one
- group_prob: float32 [2048], P(('ep', 'tp')), may hold values from 0.25 to 1
- expert_prob: float32 [2048, 2], P(('ep', 'tp')), may hold values from 0.02 to 1
- w_gate: bfloat16 [8, 2048, 1024], P('ep', None, 'tp'), may hold values from -0.125 to 0.125
- w_up: bfloat16 [8, 2048, 1024], P('ep', None, 'tp'), may hold values from -0.125 to 0.125
- w_down: bfloat16 [8, 1024, 2048], P('ep', 'tp'), may hold values from -0.1875 to 0.1875
Outputs:
- mixed: bfloat16 [1024, 2048], P(('ep', 'tp'))
- moe_out: bfloat16 [2048, 2048], P(('ep', 'tp'))
Inputs may be any that keep to these rules, and one draw needn't show every extreme that they name: `routes`: each row names 2 different experts; within the rows of one device no expert is named more than 32 times.
All inputs are finite; a program needn't handle non-finite values.
Results may differ from a plain program's by a relative error of at most 0.025.
Values may be sent and summed in bfloat16 or wider, within the bound.
A program may use at most 128 MiB of HBM per device.

v0:
```python
import functools
import math

import jax
import jax.numpy as jnp
from jax import lax
from jax.experimental import pallas as pl
from jax.experimental.pallas import tpu as pltpu
from jax.sharding import PartitionSpec as P

NOPE = 64
ROPE_DIM = 32
V_DIM = 64


epsilon = 1e-06
rope_base = 10000.0
masked_value = -1e30


def rms_scale(values, gain):
    widened = values.astype(jnp.float32)
    return widened * lax.rsqrt(jnp.mean(widened * widened, axis=-1, keepdims=True) + epsilon) * gain


def tables(positions, rope_width):
    half_width = rope_width // 2
    inverse = rope_base ** (-2.0 * jnp.arange(half_width, dtype=jnp.float32) / rope_width)
    angles = positions.astype(jnp.float32)[:, None] * inverse[None, :]
    return (jnp.cos(angles), jnp.sin(angles))


def rotate(values, cosine, sine):
    half_width = values.shape[-1] // 2
    lower = values[..., :half_width]
    upper = values[..., half_width:]
    return jnp.concatenate([lower * cosine - upper * sine, lower * sine + upper * cosine], axis=-1)


def keep_state(state_in):
    return state_in


def attend_block(running, query_rot, query_pos, key_part, value_part, rope_part):
    amount = key_part.shape[0]
    span_rows = math.gcd(amount, 1024)
    head_count = query_rot.shape[1]
    scale_factor = query_rot.shape[2] ** (-0.5)
    last_query = query_pos[-1]

    def update(state, block_at):
        row_begin = block_at * span_rows
        keys_here = lax.dynamic_slice_in_dim(key_part, row_begin, span_rows, 0).reshape(
            span_rows, head_count, -1
        )
        values_here = lax.dynamic_slice_in_dim(value_part, row_begin, span_rows, 0).reshape(
            span_rows, head_count, -1
        )
        rope_here = lax.dynamic_slice_in_dim(rope_part, row_begin, span_rows, 0)
        key_pos = row_begin + jnp.arange(span_rows, dtype=jnp.int32)

        def advance(state_in):
            top_old, totals, weighted = state_in
            shared = jnp.broadcast_to(
                rope_here[:, None, :], (span_rows, head_count, rope_here.shape[1])
            )
            full_keys = jnp.concatenate([keys_here, shared], axis=-1)
            scores = (
                jnp.einsum("qhd,khd->hqk", query_rot, full_keys, preferred_element_type=jnp.float32)
                * scale_factor
            )
            allowed = key_pos[None, :] <= query_pos[:, None]
            scores = jnp.where(allowed[None], scores, masked_value)
            top_new = jnp.maximum(top_old, jnp.max(scores, axis=-1))
            raised = jnp.where(allowed[None], jnp.exp(scores - top_new[..., None]), 0.0)
            factor = jnp.exp(top_old - top_new)
            totals = totals * factor + jnp.sum(raised, axis=-1)
            weighted = weighted * factor[..., None] + jnp.einsum(
                "hqk,khd->hqd",
                raised.astype(jnp.bfloat16),
                values_here,
                preferred_element_type=jnp.float32,
            )
            return (top_new, totals, weighted)

        return (lax.cond(key_pos[0] <= last_query, advance, keep_state, state), None)

    running, _ = lax.scan(update, running, jnp.arange(amount // span_rows))
    return running


def mixer_half(query, latent, rope_key, latent_gain, key_up, value_up, out_proj):
    query_rows = query.shape[0]
    own_rows = latent.shape[0]
    query_start = lax.axis_index("ep") * query_rows
    key_start = query_start + lax.axis_index("tp") * own_rows
    head_count = query.shape[1] // (NOPE + ROPE_DIM)
    normed = rms_scale(latent, latent_gain).astype(jnp.bfloat16)
    key_cos, key_sin = tables(key_start + jnp.arange(own_rows, dtype=jnp.int32), ROPE_DIM)
    rotated_key = rotate(rope_key.astype(jnp.float32), key_cos, key_sin).astype(jnp.bfloat16)
    query_pos = query_start + jnp.arange(query_rows, dtype=jnp.int32)
    query_cos, query_sin = tables(query_pos, ROPE_DIM)
    query_heads = query.reshape(query_rows, head_count, NOPE + ROPE_DIM)
    turned = rotate(
        query_heads[..., NOPE:].astype(jnp.float32), query_cos[:, None, :], query_sin[:, None, :]
    ).astype(jnp.bfloat16)
    query_rot = jnp.concatenate([query_heads[..., :NOPE], turned], axis=-1)
    last_query = query_start + query_rows - 1
    initial = (
        jnp.full((head_count, query_rows), masked_value, jnp.float32),
        jnp.zeros((head_count, query_rows), jnp.float32),
        jnp.zeros((head_count, query_rows, V_DIM), jnp.float32),
    )
    shard_rows = (
        lax.all_gather(normed, ("ep", "tp"), axis=0, tiled=True),
        lax.all_gather(rotated_key, ("ep", "tp"), axis=0, tiled=True),
    )

    def compute(state_in):
        key_part = jnp.dot(shard_rows[0], key_up, preferred_element_type=jnp.float32).astype(
            jnp.bfloat16
        )
        value_part = jnp.dot(shard_rows[0], value_up, preferred_element_type=jnp.float32).astype(
            jnp.bfloat16
        )
        return attend_block(state_in, query_rot, query_pos, key_part, value_part, shard_rows[1])

    running = lax.cond(jnp.int32(0) <= last_query, compute, keep_state, initial)
    totals = running[1]
    weighted = running[2]
    attention = (
        (weighted / totals[..., None])
        .transpose(1, 0, 2)
        .reshape(query_rows, head_count * V_DIM)
        .astype(jnp.bfloat16)
    )
    own_attention = lax.all_to_all(attention, "tp", split_axis=0, concat_axis=1, tiled=True)
    return jnp.dot(own_attention, out_proj, preferred_element_type=jnp.float32).astype(jnp.bfloat16)


def expert_half(tokens, moe_gain, routes, group_prob, expert_prob, w_gate, w_up, w_down):
    row_count, model_width = tokens.shape
    top_count = routes.shape[1]
    expert_count = lax.axis_size("ep")
    capacity = 2 * top_count * row_count // expert_count
    normed = rms_scale(tokens, moe_gain).astype(jnp.bfloat16)
    flat_routes = routes.reshape(-1)
    onehot = (flat_routes[:, None] == jnp.arange(expert_count, dtype=jnp.int32)[None, :]).astype(
        jnp.int32
    )
    earlier = jnp.cumsum(onehot, axis=0) - onehot
    slot_index = jnp.sum(earlier * onehot, axis=1)
    target = flat_routes * capacity + slot_index
    owner = target[None, :] == jnp.arange(expert_count * capacity, dtype=jnp.int32)[:, None]
    dispatch_table = jnp.any(
        owner.reshape(expert_count * capacity, row_count, top_count), axis=2
    ).astype(jnp.bfloat16)
    outgoing = jnp.dot(dispatch_table, normed, preferred_element_type=jnp.float32).astype(
        jnp.bfloat16
    )
    outgoing = outgoing.reshape(expert_count, capacity, model_width)
    arrived = lax.all_to_all(outgoing, "ep", split_axis=0, concat_axis=0, tiled=True)
    sources, slots, _ = arrived.shape
    flat_rows = arrived.reshape(sources * slots, model_width)
    shard_rows = lax.all_gather(flat_rows, "tp", axis=0, tiled=True)
    gate_values = jnp.dot(shard_rows, w_gate[0], preferred_element_type=jnp.float32)
    up_values = jnp.dot(shard_rows, w_up[0], preferred_element_type=jnp.float32)
    hidden = (jax.nn.silu(gate_values) * up_values).astype(jnp.bfloat16)

    def lower(offset, amount):
        return jnp.dot(hidden, w_down[0], preferred_element_type=jnp.float32)

    summed = lax.psum_scatter(
        lower(jnp.int32(0), sources * slots * lax.axis_size("tp")).astype(jnp.bfloat16),
        "tp",
        scatter_dimension=0,
        tiled=True,
    )
    result = summed.reshape(sources, slots, model_width)
    returned = lax.all_to_all(result, "ep", split_axis=0, concat_axis=0, tiled=True)
    returned_flat = returned.reshape(expert_count * capacity, model_width)
    picked = returned_flat[target].reshape(row_count, top_count, model_width).astype(jnp.float32)
    shares = group_prob[:, None] * expert_prob / jnp.sum(expert_prob, axis=1, keepdims=True)
    return jnp.sum(shares[:, :, None] * picked, axis=1).astype(jnp.bfloat16)


def body(
    query,
    latent,
    rope_key,
    latent_gain,
    key_up,
    value_up,
    out_proj,
    tokens,
    moe_gain,
    routes,
    group_prob,
    expert_prob,
    w_gate,
    w_up,
    w_down,
):
    mixed = mixer_half(query, latent, rope_key, latent_gain, key_up, value_up, out_proj)
    moe_out = expert_half(tokens, moe_gain, routes, group_prob, expert_prob, w_gate, w_up, w_down)
    return (mixed, moe_out)


def both_halves(
    heads,
    rope_width,
    outgoing,
    lat_own,
    query_big,
    key_up,
    value_up,
    out_proj_hbm,
    gate_hbm,
    up_hbm,
    down_hbm,
    slots,
    shares,
    mixed,
    moe_out,
    returned,
    relay_in,
    relay_back,
    arrived,
    lat_all,
    partial,
    from_pair,
    pair_sum,
    from_far,
    result,
    keys,
    heads_own,
    heads_all,
    out_proj,
    gate,
    up,
    down,
    load_sem,
    send_sem,
    recv_sem,
    head_send,
    head_recv,
):
    experts, capacity, width = outgoing.shape
    n_tp = lat_all.shape[2]
    depth_z = experts // 2
    middle = depth_z + 1 if depth_z == 4 else experts
    me = lax.axis_index("ep")
    tp = lax.axis_index("tp")
    me_z = me // 2
    me_y = me % 2
    mate = tp + 1 - 2 * (tp % 2)
    far = (tp + 2) % n_tp
    cross = (mate + 2) % n_tp

    loads = [
        pltpu.make_async_copy(gate_hbm, gate, load_sem.at[0]),
        pltpu.make_async_copy(up_hbm, up, load_sem.at[1]),
        pltpu.make_async_copy(down_hbm, down, load_sem.at[2]),
        pltpu.make_async_copy(out_proj_hbm, out_proj, load_sem.at[3]),
        pltpu.make_async_copy(outgoing.at[me], arrived.at[me, tp], load_sem.at[4]),
        pltpu.make_async_copy(lat_own, lat_all.at[me_z, me_y, tp], load_sem.at[5]),
    ]
    for load in loads:
        load.start()

    def remote(src, dst, kind, step, device):
        return pltpu.make_async_remote_copy(
            src_ref=src,
            dst_ref=dst,
            send_sem=send_sem.at[kind, step],
            recv_sem=recv_sem.at[kind, step],
            device_id=device,
            device_id_type=pl.DeviceIdType.MESH,
        )

    def ahead(step):
        return (me_z + step // 2) % depth_z * 2 + (me_y + step) % 2

    def behind(step):
        return (me_z + depth_z - step // 2) % depth_z * 2 + (me_y + step) % 2

    below = (me_z + depth_z - 1) % depth_z * 2
    above = (me_z + 1) % depth_z * 2
    relay_peer = below + 1 - me_y
    relay_end = below + me_y
    relay_from = above + 1 - me_y

    barrier = pltpu.get_barrier_semaphore()

    def greet(step, carry):
        pl.semaphore_signal(
            barrier,
            inc=1,
            device_id={"ep": (me + step) % experts},
            device_id_type=pl.DeviceIdType.MESH,
        )
        return carry

    lax.fori_loop(1, experts, greet, 0)
    for peer in (mate, far, cross):
        pl.semaphore_signal(
            barrier, inc=1, device_id={"tp": peer}, device_id_type=pl.DeviceIdType.MESH
        )
    pl.semaphore_wait(barrier, experts + 2)

    def ep_rows(step, slot):
        target = ahead(step)
        return remote(outgoing.at[target], arrived.at[slot, tp], 0, step, {"ep": target})

    def rows_out():
        return remote(
            outgoing.at[ahead(middle)], relay_in, 0, middle, {"ep": relay_peer}
        )

    def rows_on(slot):
        return remote(relay_in, arrived.at[slot, tp], 12, middle, {"ep": relay_end})

    def back_out():
        return remote(
            result.at[behind(middle)], relay_back, 11, middle, {"ep": relay_peer}
        )

    def back_on(slot):
        return remote(relay_back, returned.at[slot], 13, middle, {"ep": relay_end})

    def lat_x(block):
        return remote(lat_own, lat_all.at[me_z, me_y, block], 5, 0, {"tp": far})

    def lat_z(shift, part, origin):
        block = (tp + 2 * part) % n_tp
        target = (me_z + shift) % depth_z * 2 + me_y
        return remote(
            lat_all.at[me_z, me_y, block],
            lat_all.at[origin, me_y, block],
            1,
            shift * 2 + part,
            {"ep": target},
        )

    def lat_y(part, side):
        place = lat_all.at[:, side, (tp + 2 * part) % n_tp]
        return remote(place, place, 3, part, {"ep": me_z * 2 + 1 - me_y})

    def lat_mate(part, first):
        place = lat_all.at[:, :, (first + 2 * part) % n_tp]
        return remote(place, place, 7, part, {"tp": mate})

    def hop_rows(kind, step, block, peer):
        source = behind(step)
        place = arrived.at[source, block]
        return remote(place, place, kind, step, {"tp": peer})

    def to_mate(kind, step, block, part):
        source = behind(step)
        return remote(
            partial.at[source, block], from_pair.at[source, part], kind, step, {"tp": mate}
        )

    def to_far(step):
        source = behind(step)
        return remote(pair_sum.at[source], from_far.at[source], 10, step, {"tp": far})

    def back(step, slot):
        source = behind(step)
        return remote(result.at[source], returned.at[slot], 11, step, {"ep": source})

    lat_x(tp).start()
    if middle < experts:
        rows_out().start()

    def send_rows(step, carry):
        @pl.when(step != middle)
        def _():
            ep_rows(step, me).start()

        return carry

    lax.fori_loop(1, experts, send_rows, 0)
    for load in loads[4:]:
        load.wait()

    def forward(step):
        source = behind(step)

        @pl.when((step > 0) & (step != middle))
        def _():
            ep_rows(step, source).wait_recv()

        if middle < experts:

            @pl.when(step == middle)
            def _():
                rows_on(source).wait_recv()

        hop_rows(4, step, tp, far).start()
        hop_rows(2, step, tp, mate).start()

    def relay(step):
        hop_rows(4, step, far, far).wait_recv()
        hop_rows(6, step, far, mate).start()

    def compute(step):
        source = behind(step)
        hop_rows(2, step, mate, mate).wait_recv()
        hop_rows(6, step, cross, mate).wait_recv()

        @pl.when(step == 0)
        def _():
            for load in loads[:3]:
                load.wait()

        rows = arrived[source].reshape(n_tp * capacity, width)
        gate_values = jnp.dot(rows, gate[...], preferred_element_type=jnp.float32)
        up_values = jnp.dot(rows, up[...], preferred_element_type=jnp.float32)
        hidden = (gate_values / (1.0 + jnp.exp(-gate_values)) * up_values).astype(jnp.bfloat16)
        product = jnp.dot(hidden, down[...], preferred_element_type=jnp.float32)
        partial[source] = product.astype(jnp.bfloat16).reshape(n_tp, capacity, width)
        to_mate(9, step, cross, 1).start()
        to_mate(8, step, mate, 0).start()

    def reduce_pair(step):
        source = behind(step)
        to_mate(9, step, cross, 1).wait_recv()
        pair_sum[source] = (
            partial[source, far].astype(jnp.float32) + from_pair[source, 1].astype(jnp.float32)
        ).astype(jnp.bfloat16)
        to_far(step).start()

    def reduce_far(step):
        source = behind(step)
        to_mate(8, step, mate, 0).wait_recv()
        to_far(step).wait_recv()
        result[source] = (
            partial[source, tp].astype(jnp.float32)
            + from_pair[source, 0].astype(jnp.float32)
            + from_far[source].astype(jnp.float32)
        ).astype(jnp.bfloat16)

        @pl.when((step > 0) & (step != middle))
        def _():
            back(step, me).start()

        if middle < experts:

            @pl.when(step == middle)
            def _():
                back_out().start()

        @pl.when(step == 0)
        def _():
            returned[me] = result[me]

    def attend():
        rows = query_big.shape[1]
        latent_width = key_up.shape[0]
        nope_width = key_up.shape[1]
        value_width = value_up.shape[1] // heads
        packed = lat_all[...].reshape(-1, lat_all.shape[-1])
        normed = packed[:, :latent_width]
        seq = packed.shape[0]
        keys[:, :nope_width] = jnp.dot(
            normed, key_up[...], preferred_element_type=jnp.float32
        ).astype(jnp.bfloat16)
        keys[:, nope_width:] = packed[:, latent_width:]
        values = jnp.dot(normed, value_up[...], preferred_element_type=jnp.float32).astype(
            jnp.bfloat16
        )
        query_pos = me * rows + lax.broadcasted_iota(jnp.int32, (rows, seq), 0)
        allowed = lax.broadcasted_iota(jnp.int32, (rows, seq), 1) <= query_pos
        lane = lax.broadcasted_iota(jnp.int32, (rows, heads * value_width), 1)
        scale = (nope_width // heads + rope_width) ** (-0.5)
        gathered = jnp.zeros((rows, heads * value_width), jnp.float32)
        for head in range(heads):
            scores = (
                lax.dot_general(
                    query_big[head],
                    keys[...],
                    (((1,), (1,)), ((), ())),
                    preferred_element_type=jnp.float32,
                )
                * scale
            )
            scores = jnp.where(allowed, scores, masked_value)
            raised = jnp.exp(scores - jnp.max(scores, axis=1, keepdims=True))
            totals = jnp.sum(raised, axis=1, keepdims=True)
            weighted = jnp.dot(
                raised.astype(jnp.bfloat16), values, preferred_element_type=jnp.float32
            )
            inside = (lane >= head * value_width) & (lane < (head + 1) * value_width)
            gathered = jnp.where(inside, weighted / totals, gathered)
        heads_own[...] = gathered.astype(jnp.bfloat16).reshape(heads_own.shape)

    def head_copy(number, peer, slot):
        return pltpu.make_async_remote_copy(
            src_ref=heads_own.at[peer],
            dst_ref=heads_all.at[slot],
            send_sem=head_send.at[number],
            recv_sem=head_recv.at[number],
            device_id={"tp": peer},
            device_id_type=pl.DeviceIdType.MESH,
        )

    def stage(turn, carry):
        @pl.when(turn >= 4)
        def _():
            reduce_far(turn - 4)

        @pl.when((turn >= 3) & (turn < experts + 3))
        def _():
            reduce_pair(turn - 3)

        @pl.when((turn >= 2) & (turn < experts + 2))
        def _():
            compute(turn - 2)

        @pl.when((turn >= 1) & (turn < experts + 1))
        def _():
            relay(turn - 1)

        @pl.when(turn < experts)
        def _():
            forward(turn)

        @pl.when(turn == 1)
        def _():
            lat_x(far).wait_recv()

            def spread(shift, inner):
                lat_z(shift, 0, me_z).start()
                lat_z(shift, 1, me_z).start()
                return inner

            lax.fori_loop(1, depth_z, spread, 0)

        @pl.when(turn == experts - 1)
        def _():
            def collect(shift, inner):
                origin = (me_z + depth_z - shift) % depth_z
                lat_z(shift, 0, origin).wait_recv()
                lat_z(shift, 1, origin).wait_recv()
                return inner

            lax.fori_loop(1, depth_z, collect, 0)
            lat_y(0, me_y).start()
            lat_y(1, me_y).start()

        @pl.when(turn == experts + 1)
        def _():
            lat_y(0, 1 - me_y).wait_recv()
            lat_y(1, 1 - me_y).wait_recv()
            lat_mate(0, tp).start()
            lat_mate(1, tp).start()

        if middle < experts:

            @pl.when(turn == 2)
            def _():
                rows_out().wait_recv()
                rows_on(relay_from).start()

        if middle < experts:

            @pl.when(turn == experts + 2)
            def _():
                back_out().wait_recv()
                back_on(relay_from).start()

        return carry

    lax.fori_loop(0, experts + 4, stage, 0)

    lat_mate(0, mate).wait_recv()
    lat_mate(1, mate).wait_recv()
    attend()
    peers = (mate, far, cross)
    for number, peer in enumerate(peers):
        head_copy(number, peer, tp).start()
    heads_all[tp] = heads_own[tp]
    loads[3].wait()
    for number, peer in enumerate(peers):
        head_copy(number, peer, peer).wait_recv()
    depth = heads_all.shape[2]
    total = jnp.zeros(mixed.shape, jnp.float32)
    for part in range(n_tp):
        total = total + jnp.dot(
            heads_all[part],
            out_proj[part * depth : (part + 1) * depth, :],
            preferred_element_type=jnp.float32,
        )
    mixed[...] = total.astype(mixed.dtype)

    def finish(step, carry):
        @pl.when(step != middle)
        def _():
            back(step, ahead(step)).wait_recv()

        if middle < experts:

            @pl.when(step == middle)
            def _():
                back_on(ahead(middle)).wait_recv()

        return carry

    lax.fori_loop(1, experts, finish, 0)

    answers = returned[...].reshape(experts * capacity, width)
    row = lax.broadcasted_iota(jnp.int32, (slots.shape[0], experts * capacity), 1)
    chosen = jnp.zeros(moe_out.shape, jnp.float32)
    for pick in range(slots.shape[1]):
        table = jnp.where(row == slots[:, pick : pick + 1], 1.0, 0.0).astype(jnp.bfloat16)
        chosen = chosen + shares[:, pick : pick + 1] * jnp.dot(
            table, answers, preferred_element_type=jnp.float32
        )
    moe_out[...] = chosen.astype(moe_out.dtype)

    def finish_ep(step, carry):
        @pl.when(step != middle)
        def _():
            ep_rows(step, me).wait_send()
            back(step, me).wait_send()

        return carry

    lax.fori_loop(1, experts, finish_ep, 0)
    if middle < experts:
        rows_out().wait_send()
        rows_on(relay_from).wait_send()
        back_out().wait_send()
        back_on(relay_from).wait_send()
    lat_x(tp).wait_send()

    def finish_lat(shift, carry):
        lat_z(shift, 0, me_z).wait_send()
        lat_z(shift, 1, me_z).wait_send()
        return carry

    lax.fori_loop(1, depth_z, finish_lat, 0)
    for part in range(2):
        lat_y(part, me_y).wait_send()
        lat_mate(part, tp).wait_send()

    def finish_tp(step, carry):
        hop_rows(4, step, tp, far).wait_send()
        hop_rows(2, step, tp, mate).wait_send()
        hop_rows(6, step, far, mate).wait_send()
        to_mate(9, step, cross, 1).wait_send()
        to_mate(8, step, mate, 0).wait_send()
        to_far(step).wait_send()
        return carry

    lax.fori_loop(0, experts, finish_tp, 0)
    for number, peer in enumerate(peers):
        head_copy(number, peer, tp).wait_send()


def padded(amount):
    return -(-amount // 128) * 128


def fused_body(
    query,
    latent,
    rope_key,
    latent_gain,
    key_up,
    value_up,
    out_proj,
    tokens,
    moe_gain,
    routes,
    group_prob,
    expert_prob,
    w_gate,
    w_up,
    w_down,
):
    n_ep = lax.axis_size("ep")
    n_tp = lax.axis_size("tp")
    query_rows = query.shape[0]
    own_rows, latent_width = latent.shape
    query_start = lax.axis_index("ep") * query_rows
    key_start = query_start + lax.axis_index("tp") * own_rows
    heads = query.shape[1] // (NOPE + ROPE_DIM)
    normed_latent = rms_scale(latent, latent_gain).astype(jnp.bfloat16)
    key_cos, key_sin = tables(key_start + jnp.arange(own_rows, dtype=jnp.int32), ROPE_DIM)
    rotated_key = rotate(rope_key.astype(jnp.float32), key_cos, key_sin).astype(jnp.bfloat16)
    rope_room = padded(ROPE_DIM)
    gap = rope_room - ROPE_DIM
    lat_own = jnp.concatenate([normed_latent, jnp.pad(rotated_key, ((0, 0), (0, gap)))], axis=1)
    query_cos, query_sin = tables(query_start + jnp.arange(query_rows, dtype=jnp.int32), ROPE_DIM)
    query_heads = query.reshape(query_rows, heads, NOPE + ROPE_DIM).transpose(1, 0, 2)
    turned = rotate(
        query_heads[..., NOPE:].astype(jnp.float32), query_cos[None], query_sin[None]
    ).astype(jnp.bfloat16)
    own_head = jnp.eye(heads, dtype=jnp.bool_)[:, None, :, None]
    spread = jnp.where(own_head, query_heads[:, :, None, :NOPE], jnp.bfloat16(0)).reshape(
        heads, query_rows, heads * NOPE
    )
    query_big = jnp.concatenate(
        [spread, jnp.pad(turned, ((0, 0), (0, 0), (0, gap)))], axis=-1
    )

    row_count, width = tokens.shape
    top_count = routes.shape[1]
    capacity = 2 * top_count * row_count // n_ep
    normed = rms_scale(tokens, moe_gain).astype(jnp.bfloat16)
    flat_routes = routes.reshape(-1)
    onehot = (flat_routes[:, None] == jnp.arange(n_ep, dtype=jnp.int32)[None, :]).astype(jnp.int32)
    earlier = jnp.cumsum(onehot, axis=0) - onehot
    slot_index = jnp.sum(earlier * onehot, axis=1)
    target = flat_routes * capacity + slot_index
    owner = target[None, :] == jnp.arange(n_ep * capacity, dtype=jnp.int32)[:, None]
    dispatch_table = jnp.any(owner.reshape(n_ep * capacity, row_count, top_count), axis=2).astype(
        jnp.bfloat16
    )
    outgoing = jnp.dot(dispatch_table, normed, preferred_element_type=jnp.float32).astype(
        jnp.bfloat16
    )
    outgoing = outgoing.reshape(n_ep, capacity, width)

    shares = group_prob[:, None] * expert_prob / jnp.sum(expert_prob, axis=1, keepdims=True)
    bf16 = jnp.bfloat16
    lat_width = latent_width + rope_room
    vmem = pl.BlockSpec(memory_space=pltpu.VMEM)
    anywhere = pl.BlockSpec(memory_space=pl.ANY)
    mixed, moe_out = pl.pallas_call(
        functools.partial(both_halves, heads, ROPE_DIM),
        out_shape=(
            jax.ShapeDtypeStruct((own_rows, out_proj.shape[1]), bf16),
            jax.ShapeDtypeStruct((row_count, width), bf16),
        ),
        in_specs=[vmem] * 5 + [anywhere] * 4 + [vmem] * 2,
        out_specs=(vmem, vmem),
        scratch_shapes=[
            pltpu.VMEM((n_ep, capacity, width), bf16),
            pltpu.VMEM((capacity, width), bf16),
            pltpu.VMEM((capacity, width), bf16),
            pltpu.VMEM((n_ep, n_tp, capacity, width), bf16),
            pltpu.VMEM((n_ep // 2, 2, n_tp, own_rows, lat_width), bf16),
            pltpu.VMEM((n_ep, n_tp, capacity, width), bf16),
            pltpu.VMEM((n_ep, 2, capacity, width), bf16),
            pltpu.VMEM((n_ep, capacity, width), bf16),
            pltpu.VMEM((n_ep, capacity, width), bf16),
            pltpu.VMEM((n_ep, capacity, width), bf16),
            pltpu.VMEM((n_ep * n_tp * own_rows, key_up.shape[1] + rope_room), bf16),
            pltpu.VMEM((n_tp, own_rows, value_up.shape[1]), bf16),
            pltpu.VMEM((n_tp, own_rows, value_up.shape[1]), bf16),
            pltpu.VMEM(out_proj.shape, bf16),
            pltpu.VMEM(w_gate.shape[1:], bf16),
            pltpu.VMEM(w_up.shape[1:], bf16),
            pltpu.VMEM(w_down.shape[1:], bf16),
            pltpu.SemaphoreType.DMA((6,)),
            pltpu.SemaphoreType.DMA((14, n_ep)),
            pltpu.SemaphoreType.DMA((14, n_ep)),
            pltpu.SemaphoreType.DMA((3,)),
            pltpu.SemaphoreType.DMA((3,)),
        ],
        compiler_params=pltpu.CompilerParams(
            collective_id=0, has_side_effects=True, vmem_limit_bytes=56 * 1024 * 1024
        ),
        name="both_halves",
    )(
        outgoing,
        lat_own,
        query_big,
        key_up,
        value_up,
        out_proj,
        w_gate[0],
        w_up[0],
        w_down[0],
        target.reshape(row_count, top_count),
        shares,
    )
    return (mixed, moe_out)


def fits_kernel(mesh, *arrays):
    n_ep, n_tp = mesh.shape["ep"], mesh.shape["tp"]
    tokens, routes, latent = arrays[7], arrays[9], arrays[1]
    capacity = 2 * routes.shape[1] * tokens.shape[0] // (n_ep * n_tp) // n_ep
    own_rows = latent.shape[0] // (n_ep * n_tp)
    packed = latent.shape[0] <= 2048
    return n_tp == 4 and n_ep >= 8 and n_ep % 2 == 0 and capacity % 16 == 0 and own_rows % 16 == 0 and packed


def mapped(mesh, chosen):
    return jax.shard_map(
        chosen,
        mesh=mesh,
        in_specs=(
            P("ep", "tp"),
            P(("ep", "tp"), None),
            P(("ep", "tp"), None),
            P(),
            P(None, "tp"),
            P(None, "tp"),
            P(),
            P(("ep", "tp"), None),
            P(),
            P(("ep", "tp"), None),
            P(("ep", "tp")),
            P(("ep", "tp"), None),
            P("ep", None, "tp"),
            P("ep", None, "tp"),
            P("ep", "tp", None),
        ),
        out_specs=(P(("ep", "tp"), None), P(("ep", "tp"), None)),
        check_vma=False,
    )


def solution(mesh):
    def whole(*arrays):
        chosen = fused_body if fits_kernel(mesh, *arrays) else body
        return mapped(mesh, chosen)(*arrays)

    return whole
```

profile of v0, /device:TPU:0, one launch (start us, length us, event | category | flops | bytes accessed | tf_op | source)
XLA Modules:
  0.0 91.2 jit_solution(6871711346000919405)
XLA Ops:
  0.6 0.0 copy-start
  0.6 0.0 copy-start.2
  0.7 0.9 fusion.9
  1.6 1.1 %fusion.1 = f32[64]{0:T(128)S(1)} fusion(bf16[64,2048]{1,0:T(8,128)(2,1)} %param.22), kind=kLoop, calls=%fused_computation.5 | loop fusion | flops 393152 | bytes 262400 | tf_op jit(solution)/shard_map/reduce_sum | solution.py:23
  2.8 0.7 broadcast_multiply_fusion.1
  3.4 0.1 broadcast_in_dim.26
  3.5 0.1 broadcast_in_dim.27
  3.6 0.7 fusion.24
  4.3 0.1 multiply_cosine_fusion.1
  4.4 0.7 convert_element_type.51
  5.1 0.1 fusion.18
  5.3 0.1 fusion.23
  5.3 0.1 copy.49
  5.4 0.8 fusion.11
  6.3 0.6 pad_maximum_fusion.lat_own
  6.9 0.1 copy.55
  7.0 0.7 broadcast_divide_fusion.shares
  7.7 0.8 copy.48
  8.5 0.1 eq.36
  8.6 0.1 fusion.12
  8.7 0.2 reduce_window_sum.11
  8.9 0.2 select_reduce_fusion
  9.0 0.1 reduce_sum.39
  9.2 0.0 copy-start.1
  9.2 0.1 copy.50
  9.3 0.1 fusion.8
  9.4 1.0 %copy.52 = bf16[128,384]{0,1:T(8,128)(2,1)S(1)} copy(bf16[128,384]{1,0:T(8,128)(2,1)} %param.15) | data formatting | bytes 196608 | tf_op args[0]
  10.5 0.1 copy.54
  10.7 0.1 copy.53
  10.8 0.8 fusion.4.query_big
  11.6 0.0 copy-done
  11.6 0.0 copy-done.2
  11.6 1.5 %convolution_convert_fusion = bf16[256,2048]{1,0:T(8,128)(2,1)} fusion(pred[256,64]{0,1:T(8,128)(4,1)S(1)} %fusion.8, bf16[64,2048]{1,0:T(8,128)(2,1)S(1)} %copy-done, f32[2048]{0:T(1024)S(1)} %copy-done.2, f32[64]{0:T(128)S(1)} %add_rsqrt_fusion.1), kind=kOutput, calls=%fused_computation | convolution fusion | flops 68157440 | bytes 1335552 | tf_op jit(solution)/shard_map/dot_general | solution.py:722
  13.1 0.0 copy-done.1
  13.1 74.9 %both_halves.1 = (bf16[32,2048]{1,0:T(8,128)(2,1)}, bf16[64,2048]{1,0:T(8,128)(2,1)}) custom-call(bf16[8,32,2048]{2,1,0:T(8,128)(2,1)} %bitcast.9, bf16[32,640]{1,0:T(8,128)(2,1)} %pad_maximum_fusion.lat_own, bf16[4,128,384]{2,1,0:T(8,128)(2,1)} %fusion.4.query_big, bf16[512,256]{1,0:T(8,128)(2,1)} %key_up.1, bf16[512,256]{1,0:T(8,128)(2,1)} %value_up.1, ...), custom_call_target="tpu_custom_call" | custom-call | tf_op jit(solution)/shard_map/both_halves/pallas_call | solution.py:732
  88.0 1.6 %copy.59 = bf16[32,2048]{1,0:T(8,128)(2,1)} copy(bf16[32,2048]{1,0:T(8,128)(2,1)} %get-tuple-element.12) | data formatting | bytes 262144
  89.6 1.7 %copy.60 = bf16[64,2048]{1,0:T(8,128)(2,1)} copy(bf16[64,2048]{1,0:T(8,128)(2,1)} %get-tuple-element.13) | data formatting | bytes 524288
  (13 shorter events, 0.2 us)
Async XLA Ops:
  0.6 11.0 %copy-start = (bf16[64,2048]{1,0:T(8,128)(2,1)S(1)}, bf16[64,2048]{1,0:T(8,128)(2,1)}, u32[]{:S(2)}) copy-start(bf16[64,2048]{1,0:T(8,128)(2,1)} %param.22) | copy-start | bytes 786436
  0.6 11.0 %copy-start.2 = (f32[2048]{0:T(1024)S(1)}, f32[2048]{0:T(1024)}, u32[]{:S(2)}) copy-start(f32[2048]{0:T(1024)} %param.23) | copy-start | bytes 24580
  9.2 3.9 %copy-start.1 = (s32[64,2]{1,0:T(8,128)}, s32[64,2]{1,0:T(8,128)S(1)}, u32[]{:S(2)}) copy-start(s32[64,2]{1,0:T(8,128)S(1)} %add.63.slots) | copy-start | bytes 1540
where the time goes:
time: 91.7 us; the launch traced here: 91.2 us
  Pallas kernels  74.9 us (82%)
  other arithmetic  8 us (9%)
  local copies, waits for them, and re-layouts  6.06 us (7%)
  matrix products  1.49 us (2%)
    pallas_call x1, Pallas kernels, fused_body(): pl.pallas_call(functools.partial(both_halves, heads, ROPE_DIM), out_shape...  74.9 us
    unnamed x10, local copies, waits for them, and re-layouts  5.03 us
    reduce_sum x2, other arithmetic, rms_scale(): jnp.mean(widened * widened, axis=-1, keepdims=True) + epsilon  2.02 us

commit v1 on v0

v1 whole, which is shorter than its diff:
```python
import functools
import math

import jax
import jax.numpy as jnp
from jax import lax
from jax.experimental import pallas as pl
from jax.experimental.pallas import tpu as pltpu
from jax.sharding import PartitionSpec as P

NOPE = 64
ROPE_DIM = 32
V_DIM = 64


epsilon = 1e-06
rope_base = 10000.0
masked_value = -1e30


def rms_scale(values, gain):
    widened = values.astype(jnp.float32)
    return widened * lax.rsqrt(jnp.mean(widened * widened, axis=-1, keepdims=True) + epsilon) * gain


def tables(positions, rope_width):
    half_width = rope_width // 2
    inverse = rope_base ** (-2.0 * jnp.arange(half_width, dtype=jnp.float32) / rope_width)
    angles = positions.astype(jnp.float32)[:, None] * inverse[None, :]
    return (jnp.cos(angles), jnp.sin(angles))


def rotate(values, cosine, sine):
    half_width = values.shape[-1] // 2
    lower = values[..., :half_width]
    upper = values[..., half_width:]
    return jnp.concatenate([lower * cosine - upper * sine, lower * sine + upper * cosine], axis=-1)


def keep_state(state_in):
    return state_in


def attend_block(running, query_rot, query_pos, key_part, value_part, rope_part):
    amount = key_part.shape[0]
    span_rows = math.gcd(amount, 1024)
    head_count = query_rot.shape[1]
    scale_factor = query_rot.shape[2] ** (-0.5)
    last_query = query_pos[-1]

    def update(state, block_at):
        row_begin = block_at * span_rows
        keys_here = lax.dynamic_slice_in_dim(key_part, row_begin, span_rows, 0).reshape(
            span_rows, head_count, -1
        )
        values_here = lax.dynamic_slice_in_dim(value_part, row_begin, span_rows, 0).reshape(
            span_rows, head_count, -1
        )
        rope_here = lax.dynamic_slice_in_dim(rope_part, row_begin, span_rows, 0)
        key_pos = row_begin + jnp.arange(span_rows, dtype=jnp.int32)

        def advance(state_in):
            top_old, totals, weighted = state_in
            shared = jnp.broadcast_to(
                rope_here[:, None, :], (span_rows, head_count, rope_here.shape[1])
            )
            full_keys = jnp.concatenate([keys_here, shared], axis=-1)
            scores = (
                jnp.einsum("qhd,khd->hqk", query_rot, full_keys, preferred_element_type=jnp.float32)
                * scale_factor
            )
            allowed = key_pos[None, :] <= query_pos[:, None]
            scores = jnp.where(allowed[None], scores, masked_value)
            top_new = jnp.maximum(top_old, jnp.max(scores, axis=-1))
            raised = jnp.where(allowed[None], jnp.exp(scores - top_new[..., None]), 0.0)
            factor = jnp.exp(top_old - top_new)
            totals = totals * factor + jnp.sum(raised, axis=-1)
            weighted = weighted * factor[..., None] + jnp.einsum(
                "hqk,khd->hqd",
                raised.astype(jnp.bfloat16),
                values_here,
                preferred_element_type=jnp.float32,
            )
            return (top_new, totals, weighted)

        return (lax.cond(key_pos[0] <= last_query, advance, keep_state, state), None)

    running, _ = lax.scan(update, running, jnp.arange(amount // span_rows))
    return running


def mixer_half(query, latent, rope_key, latent_gain, key_up, value_up, out_proj):
    query_rows = query.shape[0]
    own_rows = latent.shape[0]
    query_start = lax.axis_index("ep") * query_rows
    key_start = query_start + lax.axis_index("tp") * own_rows
    head_count = query.shape[1] // (NOPE + ROPE_DIM)
    normed = rms_scale(latent, latent_gain).astype(jnp.bfloat16)
    key_cos, key_sin = tables(key_start + jnp.arange(own_rows, dtype=jnp.int32), ROPE_DIM)
    rotated_key = rotate(rope_key.astype(jnp.float32), key_cos, key_sin).astype(jnp.bfloat16)
    query_pos = query_start + jnp.arange(query_rows, dtype=jnp.int32)
    query_cos, query_sin = tables(query_pos, ROPE_DIM)
    query_heads = query.reshape(query_rows, head_count, NOPE + ROPE_DIM)
    turned = rotate(
        query_heads[..., NOPE:].astype(jnp.float32), query_cos[:, None, :], query_sin[:, None, :]
    ).astype(jnp.bfloat16)
    query_rot = jnp.concatenate([query_heads[..., :NOPE], turned], axis=-1)
    last_query = query_start + query_rows - 1
    initial = (
        jnp.full((head_count, query_rows), masked_value, jnp.float32),
        jnp.zeros((head_count, query_rows), jnp.float32),
        jnp.zeros((head_count, query_rows, V_DIM), jnp.float32),
    )
    shard_rows = (
        lax.all_gather(normed, ("ep", "tp"), axis=0, tiled=True),
        lax.all_gather(rotated_key, ("ep", "tp"), axis=0, tiled=True),
    )

    def compute(state_in):
        key_part = jnp.dot(shard_rows[0], key_up, preferred_element_type=jnp.float32).astype(
            jnp.bfloat16
        )
        value_part = jnp.dot(shard_rows[0], value_up, preferred_element_type=jnp.float32).astype(
            jnp.bfloat16
        )
        return attend_block(state_in, query_rot, query_pos, key_part, value_part, shard_rows[1])

    running = lax.cond(jnp.int32(0) <= last_query, compute, keep_state, initial)
    totals = running[1]
    weighted = running[2]
    attention = (
        (weighted / totals[..., None])
        .transpose(1, 0, 2)
        .reshape(query_rows, head_count * V_DIM)
        .astype(jnp.bfloat16)
    )
    own_attention = lax.all_to_all(attention, "tp", split_axis=0, concat_axis=1, tiled=True)
    return jnp.dot(own_attention, out_proj, preferred_element_type=jnp.float32).astype(jnp.bfloat16)


def expert_half(tokens, moe_gain, routes, group_prob, expert_prob, w_gate, w_up, w_down):
    row_count, model_width = tokens.shape
    top_count = routes.shape[1]
    expert_count = lax.axis_size("ep")
    capacity = 2 * top_count * row_count // expert_count
    normed = rms_scale(tokens, moe_gain).astype(jnp.bfloat16)
    flat_routes = routes.reshape(-1)
    onehot = (flat_routes[:, None] == jnp.arange(expert_count, dtype=jnp.int32)[None, :]).astype(
        jnp.int32
    )
    earlier = jnp.cumsum(onehot, axis=0) - onehot
    slot_index = jnp.sum(earlier * onehot, axis=1)
    target = flat_routes * capacity + slot_index
    owner = target[None, :] == jnp.arange(expert_count * capacity, dtype=jnp.int32)[:, None]
    dispatch_table = jnp.any(
        owner.reshape(expert_count * capacity, row_count, top_count), axis=2
    ).astype(jnp.bfloat16)
    outgoing = jnp.dot(dispatch_table, normed, preferred_element_type=jnp.float32).astype(
        jnp.bfloat16
    )
    outgoing = outgoing.reshape(expert_count, capacity, model_width)
    arrived = lax.all_to_all(outgoing, "ep", split_axis=0, concat_axis=0, tiled=True)
    sources, slots, _ = arrived.shape
    flat_rows = arrived.reshape(sources * slots, model_width)
    shard_rows = lax.all_gather(flat_rows, "tp", axis=0, tiled=True)
    gate_values = jnp.dot(shard_rows, w_gate[0], preferred_element_type=jnp.float32)
    up_values = jnp.dot(shard_rows, w_up[0], preferred_element_type=jnp.float32)
    hidden = (jax.nn.silu(gate_values) * up_values).astype(jnp.bfloat16)

    def lower(offset, amount):
        return jnp.dot(hidden, w_down[0], preferred_element_type=jnp.float32)

    summed = lax.psum_scatter(
        lower(jnp.int32(0), sources * slots * lax.axis_size("tp")).astype(jnp.bfloat16),
        "tp",
        scatter_dimension=0,
        tiled=True,
    )
    result = summed.reshape(sources, slots, model_width)
    returned = lax.all_to_all(result, "ep", split_axis=0, concat_axis=0, tiled=True)
    returned_flat = returned.reshape(expert_count * capacity, model_width)
    picked = returned_flat[target].reshape(row_count, top_count, model_width).astype(jnp.float32)
    shares = group_prob[:, None] * expert_prob / jnp.sum(expert_prob, axis=1, keepdims=True)
    return jnp.sum(shares[:, :, None] * picked, axis=1).astype(jnp.bfloat16)


def body(
    query,
    latent,
    rope_key,
    latent_gain,
    key_up,
    value_up,
    out_proj,
    tokens,
    moe_gain,
    routes,
    group_prob,
    expert_prob,
    w_gate,
    w_up,
    w_down,
):
    mixed = mixer_half(query, latent, rope_key, latent_gain, key_up, value_up, out_proj)
    moe_out = expert_half(tokens, moe_gain, routes, group_prob, expert_prob, w_gate, w_up, w_down)
    return (mixed, moe_out)


def padded(amount):
    return -(-amount // 128) * 128


def line_order(place, depth, spot):
    near = jnp.minimum(place, depth - 1 - place)
    from_low = jnp.where(spot < 2, (spot + near) % 2, spot)
    return jnp.where(place < depth // 2, from_low, depth - 1 - from_low)


def angle_tables(first_row, rows, lanes):
    half_width = ROPE_DIM // 2
    lane = lax.broadcasted_iota(jnp.int32, (rows, lanes), 1) % half_width
    position = first_row + lax.broadcasted_iota(jnp.int32, (rows, lanes), 0)
    inverse = jnp.exp(lane.astype(jnp.float32) * (-2.0 * math.log(rope_base) / ROPE_DIM))
    angles = position.astype(jnp.float32) * inverse
    return (jnp.cos(angles), jnp.sin(angles))


def turn_tables(rows, lanes, first):
    half_width = ROPE_DIM // 2
    row = lax.broadcasted_iota(jnp.int32, (rows, lanes), 0) - first
    lane = lax.broadcasted_iota(jnp.int32, (rows, lanes), 1)
    same = jnp.where((row == lane) & (lane < ROPE_DIM), 1.0, 0.0)
    lower = jnp.where((row == lane + half_width) & (lane < half_width), -1.0, 0.0)
    upper = jnp.where(
        (row == lane - half_width) & (lane >= half_width) & (lane < ROPE_DIM), 1.0, 0.0
    )
    return (same.astype(jnp.bfloat16), (lower + upper).astype(jnp.bfloat16))


def both_halves(
    heads,
    capacity,
    depth_z,
    tokens,
    moe_gain,
    routes,
    group_prob,
    expert_prob,
    latent,
    rope_key,
    latent_gain,
    query_hbm,
    key_up_hbm,
    value_up_hbm,
    out_proj_hbm,
    gate_hbm,
    up_hbm,
    down_hbm,
    mixed,
    moe_out,
    tok,
    info,
    away,
    arrived,
    lat_all,
    partial,
    from_pair,
    pair_sum,
    from_far,
    result,
    returned,
    joined,
    answers,
    passing,
    keys,
    query_big,
    heads_own,
    heads_all,
    query,
    key_up,
    value_up,
    out_proj,
    gate,
    up,
    down,
    load_sem,
    send_sem,
    recv_sem,
):
    row_count, width = tokens.shape
    own_rows, latent_width = latent.shape
    experts = 2 * depth_z
    units = 2 * depth_z
    n_tp = lat_all.shape[2]
    rope_room = lat_all.shape[-1] - latent_width
    bf16 = jnp.bfloat16
    f32 = jnp.float32
    me = lax.axis_index("ep")
    tp = lax.axis_index("tp")
    me_z = me // 2
    me_y = me % 2
    beside = me_z * 2 + 1 - me_y
    inner = (me_z > 0) & (me_z < depth_z - 1)
    inward = jnp.where(me_z < depth_z // 2, me_z + 1, me_z - 1)
    mate = tp + 1 - 2 * (tp % 2)
    far = (tp + 2) % n_tp
    cross = (mate + 2) % n_tp

    barrier = pltpu.get_barrier_semaphore()

    def greet(shift, carry):
        pl.semaphore_signal(
            barrier,
            inc=1,
            device_id={"ep": (me_z + shift) % depth_z * 2 + me_y},
            device_id_type=pl.DeviceIdType.MESH,
        )
        return carry

    lax.fori_loop(1, depth_z, greet, 0)
    pl.semaphore_signal(
        barrier, inc=1, device_id={"ep": beside}, device_id_type=pl.DeviceIdType.MESH
    )
    for peer in (mate, far, cross):
        pl.semaphore_signal(
            barrier, inc=1, device_id={"tp": peer}, device_id_type=pl.DeviceIdType.MESH
        )

    loads = [
        pltpu.make_async_copy(gate_hbm, gate, load_sem.at[0]),
        pltpu.make_async_copy(up_hbm, up, load_sem.at[1]),
        pltpu.make_async_copy(down_hbm, down, load_sem.at[2]),
        pltpu.make_async_copy(query_hbm, query, load_sem.at[3]),
        pltpu.make_async_copy(key_up_hbm, key_up, load_sem.at[4]),
        pltpu.make_async_copy(value_up_hbm, value_up, load_sem.at[5]),
        pltpu.make_async_copy(out_proj_hbm, out_proj, load_sem.at[6]),
    ]
    for load in loads:
        load.start()

    def remote(src, dst, sent, got, device):
        return pltpu.make_async_remote_copy(
            src_ref=src,
            dst_ref=dst,
            send_sem=send_sem.at[sent[0], sent[1]],
            recv_sem=recv_sem.at[got[0], got[1]],
            device_id=device,
            device_id_type=pl.DeviceIdType.MESH,
        )

    def tok_step(origin, step):
        kind = 0 if step > 0 else 1
        target = {"ep": (me_z + step) * 2 + me_y}
        return (
            remote(tok.at[origin], tok.at[origin], (kind, origin), (0, origin), target),
            remote(info.at[origin], info.at[origin], (kind + 2, origin), (2, origin), target),
        )

    def spread_tok(origin, step):
        inside = (me_z < depth_z - 1) if step > 0 else (me_z > 0)
        coming = (origin <= me_z) if step > 0 else (origin >= me_z)
        return inside & coming

    def source_of(unit):
        return line_order(me_z, depth_z, unit // 2) * 2 + (me_y + unit) % 2

    def hop_rows(kind, unit, block, peer):
        place = arrived.at[source_of(unit), block]
        return remote(place, place, (kind, unit), (kind, unit), {"tp": peer})

    def y_rows(spot):
        origin = line_order(me_z, depth_z, spot)
        return remote(
            away.at[origin],
            arrived.at[origin * 2 + me_y, tp],
            (7, spot),
            (7, spot),
            {"ep": beside},
        )

    def to_mate(kind, unit, block, part):
        source = source_of(unit)
        return remote(
            partial.at[source, block],
            from_pair.at[source, part],
            (kind, unit),
            (kind, unit),
            {"tp": mate},
        )

    def to_far(unit):
        source = source_of(unit)
        return remote(
            pair_sum.at[source], from_far.at[source], (10, unit), (10, unit), {"tp": far}
        )

    def y_back(spot):
        origin = line_order(me_z, depth_z, spot)
        return remote(
            result.at[origin * 2 + 1 - me_y],
            returned.at[origin],
            (11, spot),
            (11, spot),
            {"ep": beside},
        )

    def z_back(origin, sender):
        return remote(
            joined.at[origin],
            answers.at[sender],
            (12, origin),
            (12, sender),
            {"ep": origin * 2 + me_y},
        )

    def z_pass():
        return remote(
            joined.at[line_order(me_z, depth_z, 2)],
            passing,
            (18, 0),
            (18, 0),
            {"ep": inward * 2 + me_y},
        )

    def lat_x(block):
        place = lat_all.at[me_z, me_y, block]
        return remote(place, place, (13, 0), (13, 0), {"tp": far})

    def lat_z(shift, part, origin):
        block = (tp + 2 * part) % n_tp
        target = (me_z + shift) % depth_z * 2 + me_y
        number = shift * 2 + part
        return remote(
            lat_all.at[me_z, me_y, block],
            lat_all.at[origin, me_y, block],
            (14, number),
            (14, number),
            {"ep": target},
        )

    def lat_y(part, side):
        place = lat_all.at[:, side, (tp + 2 * part) % n_tp]
        return remote(place, place, (15, part), (15, part), {"ep": beside})

    def lat_mate(part, first):
        place = lat_all.at[:, :, (first + 2 * part) % n_tp]
        return remote(place, place, (16, part), (16, part), {"tp": mate})

    def head_copy(number, peer, slot):
        return remote(
            heads_own.at[peer], heads_all.at[slot], (17, number), (17, number), {"tp": peer}
        )

    first_route = routes[0:1, :]
    second_route = routes[1:2, :]
    lane_expert = lax.broadcasted_iota(jnp.int32, (experts, row_count), 0)
    is_first = lane_expert == first_route
    is_second = lane_expert == second_route
    named = jnp.where(is_first | is_second, 1.0, 0.0).astype(bf16)
    ahead = lax.broadcasted_iota(jnp.int32, (row_count, row_count), 0)
    behind = lax.broadcasted_iota(jnp.int32, (row_count, row_count), 1)
    before = jnp.where(ahead < behind, 1.0, 0.0).astype(bf16)
    earlier = jnp.dot(named, before, preferred_element_type=f32)
    first_slot = jnp.sum(jnp.where(is_first, earlier, 0.0), axis=0, keepdims=True)
    second_slot = jnp.sum(jnp.where(is_second, earlier, 0.0), axis=0, keepdims=True)
    both_prob = expert_prob[0:1, :] + expert_prob[1:2, :]
    info[me_z] = jnp.full(info.shape[1:], -1.0, f32)
    info[me_z, 0:1, 0:row_count] = first_route.astype(f32) * capacity + first_slot
    info[me_z, 1:2, 0:row_count] = second_route.astype(f32) * capacity + second_slot
    info[me_z, 2:3, 0:row_count] = group_prob[...] * expert_prob[0:1, :] / both_prob
    info[me_z, 3:4, 0:row_count] = group_prob[...] * expert_prob[1:2, :] / both_prob
    tok[me_z] = rms_scale(tokens[...], moe_gain[...]).astype(bf16)

    pl.semaphore_wait(barrier, depth_z + 3)

    for step in (1, -1):

        @pl.when(spread_tok(me_z, step))
        def _(step=step):
            for copy in tok_step(me_z, step):
                copy.start()

    def wanted():
        row = lax.broadcasted_iota(jnp.int32, (2 * capacity, info.shape[2]), 0)
        own = me * capacity + row
        other = (beside - 1) * capacity + row
        return jnp.where(row < capacity, own, other).astype(f32)

    def take_tok(spot):
        origin = line_order(me_z, depth_z, spot)
        for copy in tok_step(origin, 1):
            copy.wait_recv()
        for step in (1, -1):

            @pl.when(spread_tok(origin, step))
            def _(step=step):
                for copy in tok_step(origin, step):
                    copy.start()

    def gather_spot(spot):
        origin = line_order(me_z, depth_z, spot)

        @pl.when((spot > 0) & jnp.logical_not(inner))
        def _():
            take_tok(spot)

        want = wanted()
        table = jnp.where(
            (want == info[origin, 0:1, :]) | (want == info[origin, 1:2, :]), 1.0, 0.0
        )
        packed = jnp.dot(
            table[:, :row_count].astype(bf16), tok[origin], preferred_element_type=f32
        ).astype(bf16)
        arrived[origin * 2 + me_y, tp] = packed[:capacity]
        away[origin] = packed[capacity:]
        y_rows(spot).start()

    def forward(unit):
        spot = unit // 2

        @pl.when(unit % 2 == 0)
        def _():
            gather_spot(spot)

        @pl.when(unit % 2 == 1)
        def _():
            y_rows(spot).wait_recv()

        hop_rows(4, unit, tp, far).start()
        hop_rows(5, unit, tp, mate).start()

    def relay(unit):
        hop_rows(4, unit, far, far).wait_recv()
        hop_rows(6, unit, far, mate).start()

    def compute(unit):
        source = source_of(unit)
        hop_rows(5, unit, mate, mate).wait_recv()
        hop_rows(6, unit, cross, mate).wait_recv()

        @pl.when(unit == 0)
        def _():
            for load in loads[:3]:
                load.wait()

        rows = arrived[source].reshape(n_tp * capacity, width)
        gate_values = jnp.dot(rows, gate[...], preferred_element_type=f32)
        up_values = jnp.dot(rows, up[...], preferred_element_type=f32)
        hidden = (gate_values / (1.0 + jnp.exp(-gate_values)) * up_values).astype(bf16)
        product = jnp.dot(hidden, down[...], preferred_element_type=f32)
        partial[source] = product.astype(bf16).reshape(n_tp, capacity, width)
        to_mate(9, unit, cross, 1).start()
        to_mate(8, unit, mate, 0).start()

    def reduce_pair(unit):
        source = source_of(unit)
        to_mate(9, unit, cross, 1).wait_recv()
        pair_sum[source] = (
            partial[source, far].astype(f32) + from_pair[source, 1].astype(f32)
        ).astype(bf16)

    def reduce_far(unit):
        source = source_of(unit)
        to_mate(8, unit, mate, 0).wait_recv()
        to_far(unit).wait_recv()
        result[source] = (
            partial[source, tp].astype(f32)
            + from_pair[source, 0].astype(f32)
            + from_far[source].astype(f32)
        ).astype(bf16)

        @pl.when(unit % 2 == 1)
        def _():
            y_back(unit // 2).start()

    def weighted(spot):
        origin = line_order(me_z, depth_z, spot)
        y_back(spot).wait_recv()
        want = wanted()
        weights = jnp.where(want == info[origin, 0:1, :], info[origin, 2:3, :], 0.0) + jnp.where(
            want == info[origin, 1:2, :], info[origin, 3:4, :], 0.0
        )
        weights = weights[:, :row_count]
        high = weights.astype(bf16)
        low = (weights - high.astype(f32)).astype(bf16)
        rows = jnp.concatenate([result[origin * 2 + me_y], returned[origin]], axis=0)
        over_slots = (((0,), (0,)), ((), ()))
        return lax.dot_general(
            high, rows, over_slots, preferred_element_type=f32
        ) + lax.dot_general(low, rows, over_slots, preferred_element_type=f32)

    def join(spot):
        origin = line_order(me_z, depth_z, spot)
        joined[origin] = weighted(spot).astype(bf16)
        z_back(origin, me_z).start()

    def join_pass():
        origin = line_order(me_z, depth_z, 2)
        joined[origin] = weighted(2).astype(bf16)
        z_pass().start()

    def join_passed():
        origin = line_order(me_z, depth_z, 2)
        own = weighted(2)
        z_pass().wait_recv()
        joined[origin] = (own + passing[...].astype(f32)).astype(bf16)
        z_back(origin, me_z).start()

    def own_latent():
        same, swapped = turn_tables(ROPE_DIM, rope_room, 0)
        first_row = (me * n_tp + tp) * own_rows
        cosine, sine = angle_tables(first_row, own_rows, rope_room)
        turned = jnp.dot(rope_key[...], same, preferred_element_type=f32) * cosine + (
            jnp.dot(rope_key[...], swapped, preferred_element_type=f32) * sine
        )
        lat_all[me_z, me_y, tp, :, :latent_width] = rms_scale(
            latent[...], latent_gain[...]
        ).astype(bf16)
        lat_all[me_z, me_y, tp, :, latent_width:] = turned.astype(bf16)
        lat_x(tp).start()

    def spread_query():
        loads[3].wait()
        rows, packed_width = query.shape
        head_width = packed_width // heads
        nope_width = heads * NOPE
        cosine, sine = angle_tables(me * rows, rows, rope_room)
        row = lax.broadcasted_iota(jnp.int32, (packed_width, nope_width), 0)
        lane = lax.broadcasted_iota(jnp.int32, (packed_width, nope_width), 1)
        out_lane = lax.broadcasted_iota(jnp.int32, (rows, nope_width), 1)
        plain = jnp.zeros((packed_width, nope_width), f32)
        for head in range(heads):
            inside = (lane >= head * NOPE) & (lane < (head + 1) * NOPE)
            plain = jnp.where(inside & (row - lane == head * ROPE_DIM), 1.0, plain)
        nope = jnp.dot(query[...], plain.astype(bf16), preferred_element_type=f32)
        for head in range(heads):
            inside = (out_lane >= head * NOPE) & (out_lane < (head + 1) * NOPE)
            query_big[head, :, :nope_width] = jnp.where(inside, nope, 0.0).astype(bf16)
            same, swapped = turn_tables(packed_width, rope_room, head * head_width + NOPE)
            turned = jnp.dot(query[...], same, preferred_element_type=f32) * cosine + (
                jnp.dot(query[...], swapped, preferred_element_type=f32) * sine
            )
            query_big[head, :, nope_width:] = turned.astype(bf16)

    def attend():
        rows = query_big.shape[1]
        nope_width = key_up.shape[1]
        value_width = value_up.shape[1] // heads
        packed = lat_all[...].reshape(-1, lat_all.shape[-1])
        normed = packed[:, :latent_width]
        seq = packed.shape[0]
        loads[4].wait()
        loads[5].wait()
        keys[:, :nope_width] = jnp.dot(normed, key_up[...], preferred_element_type=f32).astype(bf16)
        keys[:, nope_width:] = packed[:, latent_width:]
        values = jnp.dot(normed, value_up[...], preferred_element_type=f32).astype(bf16)
        query_pos = me * rows + lax.broadcasted_iota(jnp.int32, (rows, seq), 0)
        allowed = lax.broadcasted_iota(jnp.int32, (rows, seq), 1) <= query_pos
        lane = lax.broadcasted_iota(jnp.int32, (rows, heads * value_width), 1)
        scale = (nope_width // heads + ROPE_DIM) ** (-0.5)
        gathered = jnp.zeros((rows, heads * value_width), f32)
        for head in range(heads):
            scores = (
                lax.dot_general(
                    query_big[head],
                    keys[...],
                    (((1,), (1,)), ((), ())),
                    preferred_element_type=f32,
                )
                * scale
            )
            scores = jnp.where(allowed, scores, masked_value)
            raised = jnp.exp(scores - jnp.max(scores, axis=1, keepdims=True))
            totals = jnp.sum(raised, axis=1, keepdims=True)
            summed = jnp.dot(raised.astype(bf16), values, preferred_element_type=f32)
            inside = (lane >= head * value_width) & (lane < (head + 1) * value_width)
            gathered = jnp.where(inside, summed / totals, gathered)
        heads_own[...] = gathered.astype(bf16).reshape(heads_own.shape)

    peers = (mate, far, cross)

    @pl.when(inner)
    def _():
        answers[line_order(me_z, depth_z, 3)] = jnp.zeros(answers.shape[1:], bf16)

    def stage(turn, carry):
        @pl.when((turn == 2) & inner)
        def _():
            take_tok(1)
            take_tok(2)

        @pl.when((turn == 4) & inner)
        def _():
            take_tok(3)

        @pl.when(turn < units)
        def _():
            forward(turn)

        @pl.when(turn == 0)
        def _():
            own_latent()

        @pl.when(turn == 5)
        def _():
            lat_x(far).wait_recv()

            def spread(shift, inside):
                lat_z(shift, 0, me_z).start()
                lat_z(shift, 1, me_z).start()
                return inside

            lax.fori_loop(1, depth_z, spread, 0)

        @pl.when((turn >= 1) & (turn < units + 1))
        def _():
            relay(turn - 1)

        @pl.when(turn >= 3)
        def _():
            reduce_pair(turn - 3)

            @pl.when((turn - 3 >= units - 4) & (turn - 3 < units - 2))
            def _():
                to_far(turn - 3).start()

        @pl.when((turn >= 2) & (turn < units + 2))
        def _():
            compute(turn - 2)

        @pl.when(turn == 2)
        def _():
            spread_query()

        @pl.when(turn == units)
        def _():
            def collect(shift, inside):
                origin = (me_z + depth_z - shift) % depth_z
                lat_z(shift, 0, origin).wait_recv()
                lat_z(shift, 1, origin).wait_recv()
                return inside

            lax.fori_loop(1, depth_z, collect, 0)
            lat_y(0, me_y).start()
            lat_y(1, me_y).start()

        return carry

    lax.fori_loop(0, units + 3, stage, 0)

    for unit in (7, 6, 3, 2, 1, 0):
        to_far(unit).start()

    reduce_far(4)
    reduce_far(5)
    reduce_far(7)

    @pl.when(jnp.logical_not(inner))
    def _():
        join_pass()

    lat_y(0, 1 - me_y).wait_recv()
    lat_y(1, 1 - me_y).wait_recv()
    lat_mate(0, tp).start()
    lat_mate(1, tp).start()
    reduce_far(6)
    join(3)
    lat_mate(0, mate).wait_recv()
    lat_mate(1, mate).wait_recv()
    attend()
    for number, peer in enumerate(peers):
        head_copy(number, peer, tp).start()
    heads_all[tp] = heads_own[tp]
    reduce_far(3)

    @pl.when(inner)
    def _():
        join_passed()

    reduce_far(2)
    join(1)
    reduce_far(1)
    loads[6].wait()
    for number, peer in enumerate(peers):
        head_copy(number, peer, peer).wait_recv()
    depth = heads_all.shape[2]
    total = jnp.zeros(mixed.shape, f32)
    for part in range(n_tp):
        total = total + jnp.dot(
            heads_all[part],
            out_proj[part * depth : (part + 1) * depth, :],
            preferred_element_type=f32,
        )
    mixed[...] = total.astype(mixed.dtype)
    reduce_far(0)
    chosen = weighted(0)
    for shift in range(1, depth_z):
        sender = (me_z + shift) % depth_z

        @pl.when(jnp.logical_not(inner & (sender == line_order(me_z, depth_z, 3))))
        def _(sender=sender):
            z_back(me_z, sender).wait_recv()

        chosen = chosen + answers[sender].astype(f32)
    moe_out[...] = chosen.astype(moe_out.dtype)

    def finish_line(origin, carry):
        for step in (1, -1):

            @pl.when(spread_tok(origin, step))
            def _(step=step):
                for copy in tok_step(origin, step):
                    copy.wait_send()

        y_rows(origin).wait_send()
        y_back(origin).wait_send()

        @pl.when((origin != me_z) & (inner | (origin != line_order(me_z, depth_z, 2))))
        def _():
            z_back(origin, me_z).wait_send()

        return carry

    lax.fori_loop(0, depth_z, finish_line, 0)

    @pl.when(jnp.logical_not(inner))
    def _():
        z_pass().wait_send()

    lat_x(tp).wait_send()

    def finish_lat(shift, carry):
        lat_z(shift, 0, me_z).wait_send()
        lat_z(shift, 1, me_z).wait_send()
        return carry

    lax.fori_loop(1, depth_z, finish_lat, 0)
    for part in range(2):
        lat_y(part, me_y).wait_send()
        lat_mate(part, tp).wait_send()

    def finish_tp(unit, carry):
        hop_rows(4, unit, tp, far).wait_send()
        hop_rows(5, unit, tp, mate).wait_send()
        hop_rows(6, unit, far, mate).wait_send()
        to_mate(9, unit, cross, 1).wait_send()
        to_mate(8, unit, mate, 0).wait_send()
        to_far(unit).wait_send()
        return carry

    lax.fori_loop(0, units, finish_tp, 0)
    for number, peer in enumerate(peers):
        head_copy(number, peer, tp).wait_send()


def hand_over(mixed_in, moe_in, mixed_out, moe_out):
    mixed_out[...] = mixed_in[...]
    moe_out[...] = moe_in[...]


def fused_body(
    query,
    latent,
    rope_key,
    latent_gain,
    key_up,
    value_up,
    out_proj,
    tokens,
    moe_gain,
    routes,
    group_prob,
    expert_prob,
    w_gate,
    w_up,
    w_down,
):
    n_ep = lax.axis_size("ep")
    n_tp = lax.axis_size("tp")
    depth_z = n_ep // 2
    query_rows = query.shape[0]
    own_rows, latent_width = latent.shape
    heads = query.shape[1] // (NOPE + ROPE_DIM)
    rope_room = padded(ROPE_DIM)
    row_count, width = tokens.shape
    capacity = 2 * routes.shape[1] * row_count // n_ep
    bf16 = jnp.bfloat16
    lat_width = latent_width + rope_room
    key_width = key_up.shape[1] + rope_room
    vmem = pl.BlockSpec(memory_space=pltpu.VMEM)
    anywhere = pl.BlockSpec(memory_space=pl.ANY)
    results = pl.pallas_call(
        functools.partial(both_halves, heads, capacity, depth_z),
        out_shape=(
            jax.ShapeDtypeStruct((own_rows, out_proj.shape[1]), bf16),
            jax.ShapeDtypeStruct((row_count, width), bf16),
        ),
        in_specs=[vmem] * 8 + [anywhere] * 7,
        out_specs=(vmem, vmem),
        scratch_shapes=[
            pltpu.VMEM((depth_z, row_count, width), bf16),
            pltpu.VMEM((depth_z, 8, padded(row_count)), jnp.float32),
            pltpu.VMEM((depth_z, capacity, width), bf16),
            pltpu.VMEM((n_ep, n_tp, capacity, width), bf16),
            pltpu.VMEM((depth_z, 2, n_tp, own_rows, lat_width), bf16),
            pltpu.VMEM((n_ep, n_tp, capacity, width), bf16),
            pltpu.VMEM((n_ep, 2, capacity, width), bf16),
            pltpu.VMEM((n_ep, capacity, width), bf16),
            pltpu.VMEM((n_ep, capacity, width), bf16),
            pltpu.VMEM((n_ep, capacity, width), bf16),
            pltpu.VMEM((depth_z, capacity, width), bf16),
            pltpu.VMEM((depth_z, row_count, width), bf16),
            pltpu.VMEM((depth_z, row_count, width), bf16),
            pltpu.VMEM((row_count, width), bf16),
            pltpu.VMEM((n_ep * n_tp * own_rows, key_width), bf16),
            pltpu.VMEM((heads, query_rows, key_width), bf16),
            pltpu.VMEM((n_tp, own_rows, value_up.shape[1]), bf16),
            pltpu.VMEM((n_tp, own_rows, value_up.shape[1]), bf16),
            pltpu.VMEM(query.shape, bf16),
            pltpu.VMEM(key_up.shape, bf16),
            pltpu.VMEM(value_up.shape, bf16),
            pltpu.VMEM(out_proj.shape, bf16),
            pltpu.VMEM(w_gate.shape[1:], bf16),
            pltpu.VMEM(w_up.shape[1:], bf16),
            pltpu.VMEM(w_down.shape[1:], bf16),
            pltpu.SemaphoreType.DMA((7,)),
            pltpu.SemaphoreType.DMA((19, n_ep)),
            pltpu.SemaphoreType.DMA((19, n_ep)),
        ],
        compiler_params=pltpu.CompilerParams(
            collective_id=0, has_side_effects=True, vmem_limit_bytes=60 * 1024 * 1024
        ),
        name="both_halves",
    )(
        tokens,
        moe_gain.reshape(1, -1),
        routes.T,
        group_prob.reshape(1, -1),
        expert_prob.T,
        latent,
        rope_key,
        latent_gain.reshape(1, -1),
        query,
        key_up,
        value_up,
        out_proj,
        w_gate[0],
        w_up[0],
        w_down[0],
    )
    return pl.pallas_call(
        hand_over,
        out_shape=tuple(jax.ShapeDtypeStruct(part.shape, part.dtype) for part in results),
        in_specs=[vmem] * 2,
        out_specs=(vmem, vmem),
        name="hand_over",
    )(*results)


def fits_kernel(mesh, *arrays):
    n_ep, n_tp = mesh.shape["ep"], mesh.shape["tp"]
    tokens, routes, latent = arrays[7], arrays[9], arrays[1]
    row_count = tokens.shape[0] // (n_ep * n_tp)
    capacity = 2 * routes.shape[1] * row_count // n_ep
    own_rows = latent.shape[0] // (n_ep * n_tp)
    shaped = n_tp == 4 and n_ep == 8 and routes.shape[1] == 2
    aligned = capacity % 16 == 0 and own_rows % 16 == 0 and row_count % 16 == 0
    return shaped and aligned and latent.shape[0] <= 2048


def mapped(mesh, chosen):
    return jax.shard_map(
        chosen,
        mesh=mesh,
        in_specs=(
            P("ep", "tp"),
            P(("ep", "tp"), None),
            P(("ep", "tp"), None),
            P(),
            P(None, "tp"),
            P(None, "tp"),
            P(),
            P(("ep", "tp"), None),
            P(),
            P(("ep", "tp"), None),
            P(("ep", "tp")),
            P(("ep", "tp"), None),
            P("ep", None, "tp"),
            P("ep", None, "tp"),
            P("ep", "tp", None),
        ),
        out_specs=(P(("ep", "tp"), None), P(("ep", "tp"), None)),
        check_vma=False,
    )


def solution(mesh):
    def whole(*arrays):
        chosen = fused_body if fits_kernel(mesh, *arrays) else body
        return mapped(mesh, chosen)(*arrays)

    return whole
```

time: 91.7 us -> 74.9 us (0.82)
  other arithmetic: 8 us -> 0 us
  local copies, waits for them, and re-layouts: 6.06 us -> 0 us
  matrix products: 1.49 us -> 0 us
    unnamed x10 -> x0, local copies, waits for them, and re-layouts: 5.03 us -> none
    reduce_sum x4 -> x0, other arithmetic: 2.89 us -> none  [the longest x2 2.02 us: rms_scale(): jnp.mean(widened * widened, axis=-1, keepdims=True) + epsilon]
    convert_element_type x6 -> x0, other arithmetic: 1.65 us -> none  [the longest x1 0.84 us: fused_body(): normed_latent = rms_scale(latent, latent_gain).astype(jnp.bfloat16)]
    concatenate x4 -> x0, other arithmetic: 1.49 us -> none  [the longest x1 0.79 us: fused_body(): jnp.concatenate([spread, jnp.pad(turned, ((0, 0), (0, 0), (0, gap)))], ax...]
    dot_general x1 -> x0, matrix products: 1.49 us -> none  [fused_body(): jnp.dot(dispatch_table, normed, preferred_element_type=jnp.float32)]
    pallas_call x1 -> x2, Pallas kernels: 74.9 us -> 74.1 us  [the longest x1 72.4 us: fused_body(): pl.pallas_call(functools.partial(both_halves, heads, capacity, depth_z),...]
where the time goes in v1:
time: 74.9 us; the launch traced here: 74.8 us
  Pallas kernels  74.1 us (99%)
    pallas_call x1, Pallas kernels, fused_body(): pl.pallas_call(functools.partial(both_halves, heads, capacity, depth_z),...  72.4 us
    pallas_call x1, Pallas kernels, fused_body(): pl.pallas_call(hand_over, out_shape=tuple((jax.ShapeDtypeStruct(part.shap...  1.78 us

profile of v1, /device:TPU:0, one launch (start us, length us, event | category | flops | bytes accessed | tf_op | source)
XLA Modules:
  0.0 74.8 jit_solution(11650952727072093474)
XLA Ops:
  0.6 72.4 %both_halves.1 = (bf16[32,2048]{1,0:T(8,128)(2,1)}, bf16[64,2048]{1,0:T(8,128)(2,1)}) custom-call(bf16[64,2048]{1,0:T(8,128)(2,1)} %tokens.1, f32[1,2048]{1,0:T(1,128)} %bitcast.11, s32[2,64]{1,0:T(2,128)} %bitcast.13, f32[1,64]{1,0:T(1,128)} %bitcast.15, f32[2,64]{1,0:T(2,128)} %bitcast.14, bf16[32,512]{1,0:T(8,128)(2,1)} %latent.1, ...), custom_call_target="tpu_custom_call" | custom-call | tf_op jit(solution)/shard_map/both_halves/pallas_call | solution.py:892
  73.0 1.8 %hand_over.1 = (bf16[32,2048]{1,0:T(8,128)(2,1)}, bf16[64,2048]{1,0:T(8,128)(2,1)}) custom-call(bf16[32,2048]{1,0:T(8,128)(2,1)} %get-tuple-element.4.mixed_in, bf16[64,2048]{1,0:T(8,128)(2,1)} %get-tuple-element.5.moe_in), custom_call_target="tpu_custom_call" | custom-call | tf_op jit(solution)/shard_map/hand_over/pallas_call | solution.py:951

commit v2 on v1

--- a/solution.py
+++ b/solution.py
@@ -210,10 +210,22 @@
     return -(-amount // 128) * 128
 
 
+def send_kinds(depth):
+    line = 2 * depth
+    return (line, line, depth, depth, 1, 1, 1, 1, 1, 1, 1, 1, depth, 1, line, 2, 2, 3, 2, 2)
+
+
+def recv_kinds(depth):
+    line = 2 * depth
+    units = (2 * depth,) * 3
+    return (line, 0, depth, 0, *units, depth, *units, depth, depth, 1, line, 2, 2, 3, 2, 2)
+
+
 def line_order(place, depth, spot):
-    near = jnp.minimum(place, depth - 1 - place)
-    from_low = jnp.where(spot < 2, (spot + near) % 2, spot)
-    return jnp.where(place < depth // 2, from_low, depth - 1 - from_low)
+    mirrored = depth - 1 - place
+    from_low = (place + spot) % depth
+    from_high = depth - 1 - (mirrored + spot) % depth
+    return jnp.where(place < depth // 2, from_low, from_high)
 
 
 def angle_tables(first_row, rows, lanes):
@@ -273,6 +285,7 @@
     answers,
     passing,
     keys,
+    values,
     query_big,
     heads_own,
     heads_all,
@@ -308,16 +321,17 @@
 
     barrier = pltpu.get_barrier_semaphore()
 
-    def greet(shift, carry):
-        pl.semaphore_signal(
-            barrier,
-            inc=1,
-            device_id={"ep": (me_z + shift) % depth_z * 2 + me_y},
-            device_id_type=pl.DeviceIdType.MESH,
-        )
-        return carry
-
-    lax.fori_loop(1, depth_z, greet, 0)
+    for step in (1, -1):
+
+        @pl.when((me_z + step >= 0) & (me_z + step < depth_z))
+        def _(step=step):
+            pl.semaphore_signal(
+                barrier,
+                inc=1,
+                device_id={"ep": (me_z + step) * 2 + me_y},
+                device_id_type=pl.DeviceIdType.MESH,
+            )
+
     pl.semaphore_signal(
         barrier, inc=1, device_id={"ep": beside}, device_id_type=pl.DeviceIdType.MESH
     )
@@ -342,19 +356,22 @@
         return pltpu.make_async_remote_copy(
             src_ref=src,
             dst_ref=dst,
-            send_sem=send_sem.at[sent[0], sent[1]],
-            recv_sem=recv_sem.at[got[0], got[1]],
+            send_sem=send_sem.at[sum(send_kinds(depth_z)[: sent[0]]) + sent[1]],
+            recv_sem=recv_sem.at[sum(recv_kinds(depth_z)[: got[0]]) + got[1]],
             device_id=device,
             device_id_type=pl.DeviceIdType.MESH,
         )
 
-    def tok_step(origin, step):
+    def tok_step(origin, step, half):
         kind = 0 if step > 0 else 1
         target = {"ep": (me_z + step) * 2 + me_y}
-        return (
-            remote(tok.at[origin], tok.at[origin], (kind, origin), (0, origin), target),
-            remote(info.at[origin], info.at[origin], (kind + 2, origin), (2, origin), target),
-        )
+        number = origin * 2 + half
+        place = tok.at[origin, pl.ds(half * (row_count // 2), row_count // 2)]
+        copies = [remote(place, place, (kind, number), (0, number), target)]
+        if half == 0:
+            place = info.at[origin]
+            copies.append(remote(place, place, (kind + 2, origin), (2, origin), target))
+        return copies
 
     def spread_tok(origin, step):
         inside = (me_z < depth_z - 1) if step > 0 else (me_z > 0)
@@ -366,14 +383,14 @@
 
     def hop_rows(kind, unit, block, peer):
         place = arrived.at[source_of(unit), block]
-        return remote(place, place, (kind, unit), (kind, unit), {"tp": peer})
+        return remote(place, place, (kind, 0), (kind, unit), {"tp": peer})
 
     def y_rows(spot):
         origin = line_order(me_z, depth_z, spot)
         return remote(
             away.at[origin],
             arrived.at[origin * 2 + me_y, tp],
-            (7, spot),
+            (7, 0),
             (7, spot),
             {"ep": beside},
         )
@@ -383,7 +400,7 @@
         return remote(
             partial.at[source, block],
             from_pair.at[source, part],
-            (kind, unit),
+            (kind, 0),
             (kind, unit),
             {"tp": mate},
         )
@@ -391,7 +408,7 @@
     def to_far(unit):
         source = source_of(unit)
         return remote(
-            pair_sum.at[source], from_far.at[source], (10, unit), (10, unit), {"tp": far}
+            pair_sum.at[source], from_far.at[source], (10, 0), (10, unit), {"tp": far}
         )
 
     def y_back(spot):
@@ -399,7 +416,7 @@
         return remote(
             result.at[origin * 2 + 1 - me_y],
             returned.at[origin],
-            (11, spot),
+            (11, 0),
             (11, spot),
             {"ep": beside},
         )
@@ -413,33 +430,40 @@
             {"ep": origin * 2 + me_y},
         )
 
-    def z_pass():
+    def z_pass(half):
+        rows = pl.ds(half * (row_count // 2), row_count // 2)
         return remote(
-            joined.at[line_order(me_z, depth_z, 2)],
-            passing,
-            (18, 0),
-            (18, 0),
+            joined.at[line_order(me_z, depth_z, 2), rows],
+            passing.at[rows],
+            (18, half),
+            (18, half),
             {"ep": inward * 2 + me_y},
+        )
+
+    def z_half(origin, sender, half):
+        rows = pl.ds(half * (row_count // 2), row_count // 2)
+        return remote(
+            joined.at[origin, rows],
+            answers.at[sender, rows],
+            (19, half),
+            (19, half),
+            {"ep": origin * 2 + me_y},
         )
 
     def lat_x(block):
         place = lat_all.at[me_z, me_y, block]
         return remote(place, place, (13, 0), (13, 0), {"tp": far})
 
-    def lat_z(shift, part, origin):
-        block = (tp + 2 * part) % n_tp
-        target = (me_z + shift) % depth_z * 2 + me_y
-        number = shift * 2 + part
-        return remote(
-            lat_all.at[me_z, me_y, block],
-            lat_all.at[origin, me_y, block],
-            (14, number),
-            (14, number),
-            {"ep": target},
-        )
+    def lat_up(origin):
+        copies = []
+        for part in range(2):
+            place = lat_all.at[origin, :, (tp + 2 * part) % n_tp]
+            number = (14, origin * 2 + part)
+            copies.append(remote(place, place, number, number, {"ep": (me_z + 1) * 2 + me_y}))
+        return copies
 
     def lat_y(part, side):
-        place = lat_all.at[:, side, (tp + 2 * part) % n_tp]
+        place = lat_all.at[me_z, side, (tp + 2 * part) % n_tp]
         return remote(place, place, (15, part), (15, part), {"ep": beside})
 
     def lat_mate(part, first):
@@ -471,14 +495,15 @@
     info[me_z, 3:4, 0:row_count] = group_prob[...] * expert_prob[1:2, :] / both_prob
     tok[me_z] = rms_scale(tokens[...], moe_gain[...]).astype(bf16)
 
-    pl.semaphore_wait(barrier, depth_z + 3)
+    pl.semaphore_wait(barrier, jnp.where(inner, 6, 5))
 
     for step in (1, -1):
 
         @pl.when(spread_tok(me_z, step))
         def _(step=step):
-            for copy in tok_step(me_z, step):
-                copy.start()
+            for half in range(2):
+                for copy in tok_step(me_z, step, half):
+                    copy.start()
 
     def wanted():
         row = lax.broadcasted_iota(jnp.int32, (2 * capacity, info.shape[2]), 0)
@@ -486,23 +511,37 @@
         other = (beside - 1) * capacity + row
         return jnp.where(row < capacity, own, other).astype(f32)
 
-    def take_tok(spot):
+    def take_tok(spot, half):
         origin = line_order(me_z, depth_z, spot)
-        for copy in tok_step(origin, 1):
+        for copy in tok_step(origin, 1, half):
             copy.wait_recv()
         for step in (1, -1):
 
             @pl.when(spread_tok(origin, step))
             def _(step=step):
-                for copy in tok_step(origin, step):
+                for copy in tok_step(origin, step, half):
                     copy.start()
+
+    def raise_lat(origin):
+        @pl.when(spread_tok(origin, 1))
+        def _():
+            for copy in lat_up(origin):
+                copy.start()
+
+    def take_lat(below):
+        @pl.when(me_z >= below)
+        def _():
+            for copy in lat_up(me_z - below):
+                copy.wait_recv()
+            raise_lat(me_z - below)
 
     def gather_spot(spot):
         origin = line_order(me_z, depth_z, spot)
 
         @pl.when((spot > 0) & jnp.logical_not(inner))
         def _():
-            take_tok(spot)
+            take_tok(spot, 0)
+            take_tok(spot, 1)
 
         want = wanted()
         table = jnp.where(
@@ -597,14 +636,19 @@
     def join_pass():
         origin = line_order(me_z, depth_z, 2)
         joined[origin] = weighted(2).astype(bf16)
-        z_pass().start()
+        for half in range(2):
+            z_pass(half).start()
 
     def join_passed():
-        origin = line_order(me_z, depth_z, 2)
-        own = weighted(2)
-        z_pass().wait_recv()
-        joined[origin] = (own + passing[...].astype(f32)).astype(bf16)
-        z_back(origin, me_z).start()
+        origin = line_order(me_z, depth_z, 1)
+        own = weighted(1)
+        for half in range(2):
+            first = half * (row_count // 2)
+            rows = pl.ds(first, row_count // 2)
+            z_pass(half).wait_recv()
+            part = own[first : first + row_count // 2]
+            joined[origin, rows] = (part + passing[rows].astype(f32)).astype(bf16)
+            z_half(origin, me_z, half).start()
 
     def own_latent():
         same, swapped = turn_tables(ROPE_DIM, rope_room, 0)
@@ -642,24 +686,28 @@
             )
             query_big[head, :, nope_width:] = turned.astype(bf16)
 
-    def attend():
-        rows = query_big.shape[1]
+    def fill_keys():
         nope_width = key_up.shape[1]
-        value_width = value_up.shape[1] // heads
         packed = lat_all[...].reshape(-1, lat_all.shape[-1])
         normed = packed[:, :latent_width]
-        seq = packed.shape[0]
         loads[4].wait()
         loads[5].wait()
         keys[:, :nope_width] = jnp.dot(normed, key_up[...], preferred_element_type=f32).astype(bf16)
         keys[:, nope_width:] = packed[:, latent_width:]
-        values = jnp.dot(normed, value_up[...], preferred_element_type=f32).astype(bf16)
+        values[...] = jnp.dot(normed, value_up[...], preferred_element_type=f32).astype(bf16)
+
+    def attend(first_head, last_head):
+        rows = query_big.shape[1]
+        seq = keys.shape[0]
+        value_width = values.shape[1] // heads
         query_pos = me * rows + lax.broadcasted_iota(jnp.int32, (rows, seq), 0)
         allowed = lax.broadcasted_iota(jnp.int32, (rows, seq), 1) <= query_pos
         lane = lax.broadcasted_iota(jnp.int32, (rows, heads * value_width), 1)
-        scale = (nope_width // heads + ROPE_DIM) ** (-0.5)
+        scale = (NOPE + ROPE_DIM) ** (-0.5)
         gathered = jnp.zeros((rows, heads * value_width), f32)
-        for head in range(heads):
+        if first_head > 0:
+            gathered = heads_own[...].reshape(rows, -1).astype(f32)
+        for head in range(first_head, last_head):
             scores = (
                 lax.dot_general(
                     query_big[head],
@@ -672,7 +720,7 @@
             scores = jnp.where(allowed, scores, masked_value)
             raised = jnp.exp(scores - jnp.max(scores, axis=1, keepdims=True))
             totals = jnp.sum(raised, axis=1, keepdims=True)
-            summed = jnp.dot(raised.astype(bf16), values, preferred_element_type=f32)
+            summed = jnp.dot(raised.astype(bf16), values[...], preferred_element_type=f32)
             inside = (lane >= head * value_width) & (lane < (head + 1) * value_width)
             gathered = jnp.where(inside, summed / totals, gathered)
         heads_own[...] = gathered.astype(bf16).reshape(heads_own.shape)
@@ -681,104 +729,132 @@
 
     @pl.when(inner)
     def _():
-        answers[line_order(me_z, depth_z, 3)] = jnp.zeros(answers.shape[1:], bf16)
+        answers[line_order(me_z, depth_z, 2)] = jnp.zeros(answers.shape[1:], bf16)
+
+    def clear(above, carry):
+        @pl.when(me_z + above < depth_z)
+        def _():
+            lat_all[me_z + above] = jnp.zeros(lat_all.shape[1:], bf16)
+
+        return carry
 
     def stage(turn, carry):
         @pl.when((turn == 2) & inner)
         def _():
-            take_tok(1)
-            take_tok(2)
+            take_tok(1, 1)
+            take_tok(3, 1)
 
         @pl.when((turn == 4) & inner)
         def _():
-            take_tok(3)
-
-        @pl.when(turn < units)
-        def _():
-            forward(turn)
+            take_tok(2, 1)
+
+        forward(turn)
+
+        @pl.when((turn == 1) & inner)
+        def _():
+            take_tok(1, 0)
+            take_tok(3, 0)
+
+        @pl.when((turn == 3) & inner)
+        def _():
+            take_tok(2, 0)
 
         @pl.when(turn == 0)
         def _():
             own_latent()
-
-        @pl.when(turn == 5)
+            lax.fori_loop(1, depth_z, clear, 0)
+
+        @pl.when(turn == 2)
         def _():
             lat_x(far).wait_recv()
-
-            def spread(shift, inside):
-                lat_z(shift, 0, me_z).start()
-                lat_z(shift, 1, me_z).start()
-                return inside
-
-            lax.fori_loop(1, depth_z, spread, 0)
-
-        @pl.when((turn >= 1) & (turn < units + 1))
-        def _():
-            relay(turn - 1)
-
-        @pl.when(turn >= 3)
-        def _():
-            reduce_pair(turn - 3)
-
-            @pl.when((turn - 3 >= units - 4) & (turn - 3 < units - 2))
-            def _():
-                to_far(turn - 3).start()
-
-        @pl.when((turn >= 2) & (turn < units + 2))
-        def _():
-            compute(turn - 2)
-
-        @pl.when(turn == 2)
-        def _():
-            spread_query()
-
-        @pl.when(turn == units)
-        def _():
-            def collect(shift, inside):
-                origin = (me_z + depth_z - shift) % depth_z
-                lat_z(shift, 0, origin).wait_recv()
-                lat_z(shift, 1, origin).wait_recv()
-                return inside
-
-            lax.fori_loop(1, depth_z, collect, 0)
             lat_y(0, me_y).start()
             lat_y(1, me_y).start()
 
+        @pl.when(turn == 4)
+        def _():
+            lat_y(0, 1 - me_y).wait_recv()
+            lat_y(1, 1 - me_y).wait_recv()
+            raise_lat(me_z)
+
+        @pl.when(turn == 6)
+        def _():
+            take_lat(1)
+
+        @pl.when(turn >= 3)
+        def _():
+            reduce_pair(turn - 3)
+
+        @pl.when(turn >= 2)
+        def _():
+            compute(turn - 2)
+
+        @pl.when(turn >= 1)
+        def _():
+            relay(turn - 1)
+
+        @pl.when(turn == 2)
+        def _():
+            spread_query()
+
         return carry
 
-    lax.fori_loop(0, units + 3, stage, 0)
-
-    for unit in (7, 6, 3, 2, 1, 0):
-        to_far(unit).start()
-
+    lax.fori_loop(0, units - 1, stage, 0)
+
+    reduce_pair(4)
+    to_far(4).start()
+    take_lat(2)
+    compute(5)
+    relay(6)
+    reduce_pair(5)
+    to_far(5).start()
+    forward(7)
+    to_far(3).start()
+    to_far(2).start()
+    compute(6)
     reduce_far(4)
+    reduce_pair(6)
+    take_lat(3)
+    lat_mate(0, tp).start()
+    lat_mate(1, tp).start()
     reduce_far(5)
-    reduce_far(7)
+    lat_mate(0, mate).wait_recv()
+    lat_mate(1, mate).wait_recv()
+    fill_keys()
+    relay(7)
+
+    @pl.when(inner)
+    def _():
+        join(2)
 
     @pl.when(jnp.logical_not(inner))
     def _():
         join_pass()
 
-    lat_y(0, 1 - me_y).wait_recv()
-    lat_y(1, 1 - me_y).wait_recv()
-    lat_mate(0, tp).start()
-    lat_mate(1, tp).start()
-    reduce_far(6)
-    join(3)
-    lat_mate(0, mate).wait_recv()
-    lat_mate(1, mate).wait_recv()
-    attend()
+    compute(7)
+    reduce_pair(7)
+    to_far(7).start()
+    to_far(6).start()
+    reduce_far(3)
+    attend(0, heads // 2)
+    reduce_far(2)
+    attend(heads // 2, heads)
     for number, peer in enumerate(peers):
         head_copy(number, peer, tp).start()
+    to_far(1).start()
+    to_far(0).start()
     heads_all[tp] = heads_own[tp]
-    reduce_far(3)
+    reduce_far(7)
 
     @pl.when(inner)
     def _():
         join_passed()
 
-    reduce_far(2)
-    join(1)
+    @pl.when(jnp.logical_not(inner))
+    def _():
+        join(1)
+
+    reduce_far(6)
+    join(3)
     reduce_far(1)
     loads[6].wait()
     for number, peer in enumerate(peers):
@@ -794,28 +870,23 @@
     mixed[...] = total.astype(mixed.dtype)
     reduce_far(0)
     chosen = weighted(0)
-    for shift in range(1, depth_z):
-        sender = (me_z + shift) % depth_z
-
-        @pl.when(jnp.logical_not(inner & (sender == line_order(me_z, depth_z, 3))))
-        def _(sender=sender):
-            z_back(me_z, sender).wait_recv()
-
-        chosen = chosen + answers[sender].astype(f32)
-    moe_out[...] = chosen.astype(moe_out.dtype)
 
     def finish_line(origin, carry):
         for step in (1, -1):
 
             @pl.when(spread_tok(origin, step))
             def _(step=step):
-                for copy in tok_step(origin, step):
+                for copy in (*tok_step(origin, step, 0), *tok_step(origin, step, 1)):
                     copy.wait_send()
 
-        y_rows(origin).wait_send()
-        y_back(origin).wait_send()
-
-        @pl.when((origin != me_z) & (inner | (origin != line_order(me_z, depth_z, 2))))
+        @pl.when(spread_tok(origin, 1))
+        def _():
+            for copy in lat_up(origin):
+                copy.wait_send()
+
+        halved = jnp.where(inner, line_order(me_z, depth_z, 1), line_order(me_z, depth_z, 2))
+
+        @pl.when((origin != me_z) & (origin != halved))
         def _():
             z_back(origin, me_z).wait_send()
 
@@ -825,37 +896,61 @@
 
     @pl.when(jnp.logical_not(inner))
     def _():
-        z_pass().wait_send()
+        for half in range(2):
+            z_pass(half).wait_send()
+
+    @pl.when(inner)
+    def _():
+        for half in range(2):
+            z_half(line_order(me_z, depth_z, 1), me_z, half).wait_send()
 
     lat_x(tp).wait_send()
-
-    def finish_lat(shift, carry):
-        lat_z(shift, 0, me_z).wait_send()
-        lat_z(shift, 1, me_z).wait_send()
-        return carry
-
-    lax.fori_loop(1, depth_z, finish_lat, 0)
     for part in range(2):
         lat_y(part, me_y).wait_send()
         lat_mate(part, tp).wait_send()
-
-    def finish_tp(unit, carry):
-        hop_rows(4, unit, tp, far).wait_send()
-        hop_rows(5, unit, tp, mate).wait_send()
-        hop_rows(6, unit, far, mate).wait_send()
-        to_mate(9, unit, cross, 1).wait_send()
-        to_mate(8, unit, mate, 0).wait_send()
-        to_far(unit).wait_send()
-        return carry
-
-    lax.fori_loop(0, units, finish_tp, 0)
     for number, peer in enumerate(peers):
         head_copy(number, peer, tp).wait_send()
 
-
-def hand_over(mixed_in, moe_in, mixed_out, moe_out):
-    mixed_out[...] = mixed_in[...]
-    moe_out[...] = moe_in[...]
+    def all_sent(kind, src, device):
+        remote(src, src, (kind, 0), (4, 0), device).wait_send()
+
+    all_sent(4, arrived.at[:, tp], {"tp": far})
+    all_sent(5, arrived.at[:, tp], {"tp": mate})
+    all_sent(6, arrived.at[:, far], {"tp": mate})
+    all_sent(7, away, {"ep": beside})
+    all_sent(8, partial.at[:, mate], {"tp": mate})
+    all_sent(9, partial.at[:, cross], {"tp": mate})
+    all_sent(10, pair_sum, {"tp": far})
+    all_sent(11, returned, {"ep": beside})
+
+    for shift in range(1, depth_z):
+        sender = (me_z + shift) % depth_z
+
+        near = line_order(me_z, depth_z, 1)
+        none = line_order(me_z, depth_z, 2)
+
+        @pl.when(jnp.logical_not(inner & ((sender == none) | (sender == near))))
+        def _(sender=sender):
+            z_back(me_z, sender).wait_recv()
+
+        @pl.when(inner & (sender == near))
+        def _(sender=sender):
+            for half in range(2):
+                z_half(me_z, sender, half).wait_recv()
+
+        chosen = chosen + answers[sender].astype(f32)
+    moe_out[...] = chosen.astype(moe_out.dtype)
+
+
+def hand_over(mixed_in, moe_in, mixed_out, moe_out, sem):
+    copies = [
+        pltpu.make_async_copy(mixed_in, mixed_out, sem.at[0]),
+        pltpu.make_async_copy(moe_in, moe_out, sem.at[1]),
+    ]
+    for copy in copies:
+        copy.start()
+    for copy in copies:
+        copy.wait()
 
 
 def fused_body(
@@ -892,8 +987,8 @@
     results = pl.pallas_call(
         functools.partial(both_halves, heads, capacity, depth_z),
         out_shape=(
-            jax.ShapeDtypeStruct((own_rows, out_proj.shape[1]), bf16),
-            jax.ShapeDtypeStruct((row_count, width), bf16),
+            pltpu.VMEM((own_rows, out_proj.shape[1]), bf16),
+            pltpu.VMEM((row_count, width), bf16),
         ),
         in_specs=[vmem] * 8 + [anywhere] * 7,
         out_specs=(vmem, vmem),
@@ -913,6 +1008,7 @@
             pltpu.VMEM((depth_z, row_count, width), bf16),
             pltpu.VMEM((row_count, width), bf16),
             pltpu.VMEM((n_ep * n_tp * own_rows, key_width), bf16),
+            pltpu.VMEM((n_ep * n_tp * own_rows, value_up.shape[1]), bf16),
             pltpu.VMEM((heads, query_rows, key_width), bf16),
             pltpu.VMEM((n_tp, own_rows, value_up.shape[1]), bf16),
             pltpu.VMEM((n_tp, own_rows, value_up.shape[1]), bf16),
@@ -924,8 +1020,8 @@
             pltpu.VMEM(w_up.shape[1:], bf16),
             pltpu.VMEM(w_down.shape[1:], bf16),
             pltpu.SemaphoreType.DMA((7,)),
-            pltpu.SemaphoreType.DMA((19, n_ep)),
-            pltpu.SemaphoreType.DMA((19, n_ep)),
+            pltpu.SemaphoreType.DMA((sum(send_kinds(depth_z)),)),
+            pltpu.SemaphoreType.DMA((sum(recv_kinds(depth_z)),)),
         ],
         compiler_params=pltpu.CompilerParams(
             collective_id=0, has_side_effects=True, vmem_limit_bytes=60 * 1024 * 1024
@@ -952,7 +1048,9 @@
         hand_over,
         out_shape=tuple(jax.ShapeDtypeStruct(part.shape, part.dtype) for part in results),
         in_specs=[vmem] * 2,
-        out_specs=(vmem, vmem),
+        out_specs=(anywhere, anywhere),
+        scratch_shapes=[pltpu.SemaphoreType.DMA((2,))],
+        compiler_params=pltpu.CompilerParams(vmem_limit_bytes=4 * 1024 * 1024),
         name="hand_over",
     )(*results)
 

time: 74.9 us -> 69.3 us (0.925)
  Pallas kernels: 74.1 us -> 68.5 us
    pallas_call x1, Pallas kernels: 72.4 us -> 67.7 us  [fused_body(): pl.pallas_call(functools.partial(both_halves, heads, capacity, depth_z),...]
    pallas_call x1, Pallas kernels: 1.78 us -> 0.77 us  [fused_body(): pl.pallas_call(hand_over, out_shape=tuple((jax.ShapeDtypeStruct(part.shap...]
where the time goes in v2:
time: 69.3 us; the launch traced here: 69.1 us
  Pallas kernels  68.5 us (99%)
    pallas_call x1, Pallas kernels, fused_body(): pl.pallas_call(functools.partial(both_halves, heads, capacity, depth_z),...  67.7 us

profile of v2, /device:TPU:0, one launch (start us, length us, event | category | flops | bytes accessed | tf_op | source)
XLA Modules:
  0.0 69.1 jit_solution(1706661454449773244)
XLA Ops:
  0.6 67.7 %both_halves.1 = (bf16[32,2048]{1,0:T(8,128)(2,1)S(1)}, bf16[64,2048]{1,0:T(8,128)(2,1)S(1)}) custom-call(bf16[64,2048]{1,0:T(8,128)(2,1)} %tokens.1, f32[1,2048]{1,0:T(1,128)} %bitcast.11, s32[2,64]{1,0:T(2,128)} %bitcast.13, f32[1,64]{1,0:T(1,128)} %bitcast.15, f32[2,64]{1,0:T(2,128)} %bitcast.14, bf16[32,512]{1,0:T(8,128)(2,1)} %latent.1, ...), custom_call_target="tpu_custom_call" | custom-call | tf_op jit(solution)/shard_map/both_halves/pallas_call | solution.py:987
  68.4 0.8 %hand_over.1 = (bf16[32,2048]{1,0:T(8,128)(2,1)}, bf16[64,2048]{1,0:T(8,128)(2,1)}) custom-call(bf16[32,2048]{1,0:T(8,128)(2,1)S(1)} %get-tuple-element.4.mixed_in, bf16[64,2048]{1,0:T(8,128)(2,1)S(1)} %get-tuple-element.5.moe_in), custom_call_target="tpu_custom_call" | custom-call | tf_op jit(solution)/shard_map/hand_over/pallas_call | solution.py:1047

commit v3 on v2

--- a/solution.py
+++ b/solution.py
@@ -212,13 +212,14 @@
 
 def send_kinds(depth):
     line = 2 * depth
-    return (line, line, depth, depth, 1, 1, 1, 1, 1, 1, 1, 1, depth, 1, line, 2, 2, 3, 2, 2)
+    return (line, line, depth, depth, 1, 1, 1, 1, 1, 1, 1, 1, line, 1, line, 2, 2, 3, 2)
 
 
 def recv_kinds(depth):
     line = 2 * depth
-    units = (2 * depth,) * 3
-    return (line, 0, depth, 0, *units, depth, *units, depth, depth, 1, line, 2, 2, 3, 2, 2)
+    wide = 2 * line
+    gather = (wide, line, line, line, line, line, wide)
+    return (line, 0, depth, 0, *gather, line, line, 1, line, 2, 2, 3, 2)
 
 
 def line_order(place, depth, spot):
@@ -362,11 +363,14 @@
             device_id_type=pl.DeviceIdType.MESH,
         )
 
+    def columns(half):
+        return pl.ds(half * (width // 2), width // 2)
+
     def tok_step(origin, step, half):
         kind = 0 if step > 0 else 1
         target = {"ep": (me_z + step) * 2 + me_y}
         number = origin * 2 + half
-        place = tok.at[origin, pl.ds(half * (row_count // 2), row_count // 2)]
+        place = tok.at[origin, :, columns(half)]
         copies = [remote(place, place, (kind, number), (0, number), target)]
         if half == 0:
             place = info.at[origin]
@@ -385,13 +389,17 @@
         place = arrived.at[source_of(unit), block]
         return remote(place, place, (kind, 0), (kind, unit), {"tp": peer})
 
-    def y_rows(spot):
+    def far_rows(unit, half, block):
+        place = arrived.at[source_of(unit), block, :, columns(half)]
+        return remote(place, place, (4, 0), (4, unit * 2 + half), {"tp": far})
+
+    def y_rows(spot, half):
         origin = line_order(me_z, depth_z, spot)
         return remote(
-            away.at[origin],
-            arrived.at[origin * 2 + me_y, tp],
+            away.at[origin, :, columns(half)],
+            arrived.at[origin * 2 + me_y, tp, :, columns(half)],
             (7, 0),
-            (7, spot),
+            (7, spot * 2 + half),
             {"ep": beside},
         )
 
@@ -405,49 +413,46 @@
             {"tp": mate},
         )
 
-    def to_far(unit):
+    def to_far(unit, half):
         source = source_of(unit)
         return remote(
-            pair_sum.at[source], from_far.at[source], (10, 0), (10, unit), {"tp": far}
-        )
-
-    def y_back(spot):
+            pair_sum.at[source, :, columns(half)],
+            from_far.at[source, :, columns(half)],
+            (10, 0),
+            (10, unit * 2 + half),
+            {"tp": far},
+        )
+
+    def send_far(unit):
+        for half in range(2):
+            to_far(unit, half).start()
+
+    def y_back(spot, half):
         origin = line_order(me_z, depth_z, spot)
         return remote(
-            result.at[origin * 2 + 1 - me_y],
-            returned.at[origin],
+            result.at[origin * 2 + 1 - me_y, :, columns(half)],
+            returned.at[origin, :, columns(half)],
             (11, 0),
-            (11, spot),
+            (11, spot * 2 + half),
             {"ep": beside},
         )
 
-    def z_back(origin, sender):
+    def z_back(origin, sender, half):
         return remote(
-            joined.at[origin],
-            answers.at[sender],
-            (12, origin),
-            (12, sender),
+            joined.at[origin, :, columns(half)],
+            answers.at[sender, :, columns(half)],
+            (12, origin * 2 + half),
+            (12, sender * 2 + half),
             {"ep": origin * 2 + me_y},
         )
 
     def z_pass(half):
-        rows = pl.ds(half * (row_count // 2), row_count // 2)
         return remote(
-            joined.at[line_order(me_z, depth_z, 2), rows],
-            passing.at[rows],
+            joined.at[line_order(me_z, depth_z, 2), :, columns(half)],
+            passing.at[:, columns(half)],
             (18, half),
             (18, half),
             {"ep": inward * 2 + me_y},
-        )
-
-    def z_half(origin, sender, half):
-        rows = pl.ds(half * (row_count // 2), row_count // 2)
-        return remote(
-            joined.at[origin, rows],
-            answers.at[sender, rows],
-            (19, half),
-            (19, half),
-            {"ep": origin * 2 + me_y},
         )
 
     def lat_x(block):
@@ -535,41 +540,37 @@
                 copy.wait_recv()
             raise_lat(me_z - below)
 
-    def gather_spot(spot):
+    def gather_spot(spot, half):
         origin = line_order(me_z, depth_z, spot)
 
         @pl.when((spot > 0) & jnp.logical_not(inner))
         def _():
-            take_tok(spot, 0)
-            take_tok(spot, 1)
+            take_tok(spot, half)
 
         want = wanted()
         table = jnp.where(
             (want == info[origin, 0:1, :]) | (want == info[origin, 1:2, :]), 1.0, 0.0
         )
         packed = jnp.dot(
-            table[:, :row_count].astype(bf16), tok[origin], preferred_element_type=f32
+            table[:, :row_count].astype(bf16),
+            tok[origin, :, columns(half)],
+            preferred_element_type=f32,
         ).astype(bf16)
-        arrived[origin * 2 + me_y, tp] = packed[:capacity]
-        away[origin] = packed[capacity:]
-        y_rows(spot).start()
-
-    def forward(unit):
-        spot = unit // 2
-
-        @pl.when(unit % 2 == 0)
-        def _():
-            gather_spot(spot)
-
-        @pl.when(unit % 2 == 1)
-        def _():
-            y_rows(spot).wait_recv()
-
-        hop_rows(4, unit, tp, far).start()
+        arrived[origin * 2 + me_y, tp, :, columns(half)] = packed[:capacity]
+        away[origin, :, columns(half)] = packed[capacity:]
+        y_rows(spot, half).start()
+        far_rows(spot * 2, half, tp).start()
+
+    def pass_y(spot, half):
+        y_rows(spot, half).wait_recv()
+        far_rows(spot * 2 + 1, half, tp).start()
+
+    def share(unit):
         hop_rows(5, unit, tp, mate).start()
 
     def relay(unit):
-        hop_rows(4, unit, far, far).wait_recv()
+        for half in range(2):
+            far_rows(unit, half, far).wait_recv()
         hop_rows(6, unit, far, mate).start()
 
     def compute(unit):
@@ -601,20 +602,19 @@
     def reduce_far(unit):
         source = source_of(unit)
         to_mate(8, unit, mate, 0).wait_recv()
-        to_far(unit).wait_recv()
-        result[source] = (
-            partial[source, tp].astype(f32)
-            + from_pair[source, 0].astype(f32)
-            + from_far[source].astype(f32)
-        ).astype(bf16)
-
-        @pl.when(unit % 2 == 1)
-        def _():
-            y_back(unit // 2).start()
-
-    def weighted(spot):
+        for half in range(2):
+            to_far(unit, half).wait_recv()
+            result[source, :, columns(half)] = (
+                partial[source, tp, :, columns(half)].astype(f32)
+                + from_pair[source, 0, :, columns(half)].astype(f32)
+                + from_far[source, :, columns(half)].astype(f32)
+            ).astype(bf16)
+            if unit % 2 == 1:
+                y_back(unit // 2, half).start()
+
+    def weighted(spot, half):
         origin = line_order(me_z, depth_z, spot)
-        y_back(spot).wait_recv()
+        y_back(spot, half).wait_recv()
         want = wanted()
         weights = jnp.where(want == info[origin, 0:1, :], info[origin, 2:3, :], 0.0) + jnp.where(
             want == info[origin, 1:2, :], info[origin, 3:4, :], 0.0
@@ -622,7 +622,10 @@
         weights = weights[:, :row_count]
         high = weights.astype(bf16)
         low = (weights - high.astype(f32)).astype(bf16)
-        rows = jnp.concatenate([result[origin * 2 + me_y], returned[origin]], axis=0)
+        rows = jnp.concatenate(
+            [result[origin * 2 + me_y, :, columns(half)], returned[origin, :, columns(half)]],
+            axis=0,
+        )
         over_slots = (((0,), (0,)), ((), ()))
         return lax.dot_general(
             high, rows, over_slots, preferred_element_type=f32
@@ -630,25 +633,25 @@
 
     def join(spot):
         origin = line_order(me_z, depth_z, spot)
-        joined[origin] = weighted(spot).astype(bf16)
-        z_back(origin, me_z).start()
+        for half in range(2):
+            joined[origin, :, columns(half)] = weighted(spot, half).astype(bf16)
+            z_back(origin, me_z, half).start()
 
     def join_pass():
         origin = line_order(me_z, depth_z, 2)
-        joined[origin] = weighted(2).astype(bf16)
         for half in range(2):
+            joined[origin, :, columns(half)] = weighted(2, half).astype(bf16)
             z_pass(half).start()
 
     def join_passed():
         origin = line_order(me_z, depth_z, 1)
-        own = weighted(1)
         for half in range(2):
-            first = half * (row_count // 2)
-            rows = pl.ds(first, row_count // 2)
+            own = weighted(1, half)
             z_pass(half).wait_recv()
-            part = own[first : first + row_count // 2]
-            joined[origin, rows] = (part + passing[rows].astype(f32)).astype(bf16)
-            z_half(origin, me_z, half).start()
+            joined[origin, :, columns(half)] = (
+                own + passing[:, columns(half)].astype(f32)
+            ).astype(bf16)
+            z_back(origin, me_z, half).start()
 
     def own_latent():
         same, swapped = turn_tables(ROPE_DIM, rope_room, 0)
@@ -739,30 +742,58 @@
         return carry
 
     def stage(turn, carry):
+        spot = turn // 2
+
+        @pl.when(turn == 0)
+        def _():
+            gather_spot(0, 0)
+
+        @pl.when(turn == 1)
+        def _():
+            pass_y(0, 1)
+
+        @pl.when((turn == 1) & inner)
+        def _():
+            take_tok(1, 0)
+            take_tok(3, 0)
+
         @pl.when((turn == 2) & inner)
         def _():
             take_tok(1, 1)
             take_tok(3, 1)
 
+        @pl.when((turn == 3) & inner)
+        def _():
+            take_tok(2, 0)
+
         @pl.when((turn == 4) & inner)
         def _():
             take_tok(2, 1)
 
-        forward(turn)
-
-        @pl.when((turn == 1) & inner)
-        def _():
-            take_tok(1, 0)
-            take_tok(3, 0)
-
-        @pl.when((turn == 3) & inner)
-        def _():
-            take_tok(2, 0)
+        @pl.when(turn % 2 == 0)
+        def _():
+            gather_spot(spot, 1)
+            share(turn)
+
+            @pl.when(turn > 0)
+            def _():
+                pass_y(spot, 0)
+
+        @pl.when(turn % 2 == 1)
+        def _():
+            gather_spot(spot + 1, 0)
+
+            @pl.when(turn > 1)
+            def _():
+                pass_y(spot, 1)
+
+            share(turn)
 
         @pl.when(turn == 0)
         def _():
             own_latent()
             lax.fori_loop(1, depth_z, clear, 0)
+            pass_y(0, 0)
 
         @pl.when(turn == 2)
         def _():
@@ -780,9 +811,9 @@
         def _():
             take_lat(1)
 
-        @pl.when(turn >= 3)
-        def _():
-            reduce_pair(turn - 3)
+        @pl.when(turn >= 4)
+        def _():
+            reduce_pair(turn - 4)
 
         @pl.when(turn >= 2)
         def _():
@@ -800,27 +831,41 @@
 
     lax.fori_loop(0, units - 1, stage, 0)
 
+    pass_y(depth_z - 1, 1)
+    share(7)
     reduce_pair(4)
-    to_far(4).start()
+    send_far(4)
     take_lat(2)
     compute(5)
     relay(6)
+    reduce_pair(3)
     reduce_pair(5)
-    to_far(5).start()
-    forward(7)
-    to_far(3).start()
-    to_far(2).start()
+    send_far(5)
     compute(6)
-    reduce_far(4)
-    reduce_pair(6)
     take_lat(3)
     lat_mate(0, tp).start()
     lat_mate(1, tp).start()
-    reduce_far(5)
+    reduce_pair(6)
+    relay(7)
     lat_mate(0, mate).wait_recv()
     lat_mate(1, mate).wait_recv()
     fill_keys()
-    relay(7)
+    compute(7)
+    send_far(3)
+    reduce_far(4)
+    reduce_far(5)
+    reduce_pair(7)
+    send_far(7)
+    send_far(6)
+    attend(0, heads // 2)
+    attend(heads // 2, heads)
+    for number, peer in enumerate(peers):
+        head_copy(number, peer, tp).start()
+    send_far(2)
+    send_far(1)
+    send_far(0)
+    heads_all[tp] = heads_own[tp]
+    reduce_far(3)
 
     @pl.when(inner)
     def _():
@@ -830,20 +875,11 @@
     def _():
         join_pass()
 
-    compute(7)
-    reduce_pair(7)
-    to_far(7).start()
-    to_far(6).start()
-    reduce_far(3)
-    attend(0, heads // 2)
+    reduce_far(7)
+    reduce_far(6)
+
+    join(3)
     reduce_far(2)
-    attend(heads // 2, heads)
-    for number, peer in enumerate(peers):
-        head_copy(number, peer, tp).start()
-    to_far(1).start()
-    to_far(0).start()
-    heads_all[tp] = heads_own[tp]
-    reduce_far(7)
 
     @pl.when(inner)
     def _():
@@ -853,9 +889,6 @@
     def _():
         join(1)
 
-    reduce_far(6)
-    join(3)
-    reduce_far(1)
     loads[6].wait()
     for number, peer in enumerate(peers):
         head_copy(number, peer, peer).wait_recv()
@@ -868,8 +901,9 @@
             preferred_element_type=f32,
         )
     mixed[...] = total.astype(mixed.dtype)
+    reduce_far(1)
     reduce_far(0)
-    chosen = weighted(0)
+    chosen = [weighted(0, half) for half in range(2)]
 
     def finish_line(origin, carry):
         for step in (1, -1):
@@ -884,11 +918,12 @@
             for copy in lat_up(origin):
                 copy.wait_send()
 
-        halved = jnp.where(inner, line_order(me_z, depth_z, 1), line_order(me_z, depth_z, 2))
-
-        @pl.when((origin != me_z) & (origin != halved))
-        def _():
-            z_back(origin, me_z).wait_send()
+        passed = jnp.logical_not(inner) & (origin == line_order(me_z, depth_z, 2))
+
+        @pl.when((origin != me_z) & jnp.logical_not(passed))
+        def _():
+            for half in range(2):
+                z_back(origin, me_z, half).wait_send()
 
         return carry
 
@@ -898,11 +933,6 @@
     def _():
         for half in range(2):
             z_pass(half).wait_send()
-
-    @pl.when(inner)
-    def _():
-        for half in range(2):
-            z_half(line_order(me_z, depth_z, 1), me_z, half).wait_send()
 
     lat_x(tp).wait_send()
     for part in range(2):
@@ -923,23 +953,18 @@
     all_sent(10, pair_sum, {"tp": far})
     all_sent(11, returned, {"ep": beside})
 
-    for shift in range(1, depth_z):
-        sender = (me_z + shift) % depth_z
-
-        near = line_order(me_z, depth_z, 1)
-        none = line_order(me_z, depth_z, 2)
-
-        @pl.when(jnp.logical_not(inner & ((sender == none) | (sender == near))))
-        def _(sender=sender):
-            z_back(me_z, sender).wait_recv()
-
-        @pl.when(inner & (sender == near))
-        def _(sender=sender):
-            for half in range(2):
-                z_half(me_z, sender, half).wait_recv()
-
-        chosen = chosen + answers[sender].astype(f32)
-    moe_out[...] = chosen.astype(moe_out.dtype)
+    none = line_order(me_z, depth_z, 2)
+    for half in range(2):
+        total = chosen[half]
+        for shift in range(1, depth_z):
+            sender = (me_z + shift) % depth_z
+
+            @pl.when(jnp.logical_not(inner & (sender == none)))
+            def _(sender=sender, half=half):
+                z_back(me_z, sender, half).wait_recv()
+
+            total = total + answers[sender, :, columns(half)].astype(f32)
+        moe_out[:, columns(half)] = total.astype(moe_out.dtype)
 
 
 def hand_over(mixed_in, moe_in, mixed_out, moe_out, sem):

time: 69.3 us -> 63.7 us (0.919)
  Pallas kernels: 68.5 us -> 62.6 us
    pallas_call x1, Pallas kernels: 67.7 us -> 61.8 us  [fused_body(): pl.pallas_call(functools.partial(both_halves, heads, capacity, depth_z),...]
where the time goes in v3:
time: 63.7 us; the launch traced here: 63.2 us
  Pallas kernels  62.6 us (98%)
  between operations  0.64 us (1%)
    pallas_call x1, Pallas kernels, fused_body(): pl.pallas_call(functools.partial(both_halves, heads, capacity, depth_z),...  61.8 us

profile of v3, /device:TPU:0, one launch (start us, length us, event | category | flops | bytes accessed | tf_op | source)
XLA Modules:
  0.0 63.2 jit_solution(14030838975130386316)
XLA Ops:
  0.6 61.8 %both_halves.1 = (bf16[32,2048]{1,0:T(8,128)(2,1)S(1)}, bf16[64,2048]{1,0:T(8,128)(2,1)S(1)}) custom-call(bf16[64,2048]{1,0:T(8,128)(2,1)} %tokens.1, f32[1,2048]{1,0:T(1,128)} %bitcast.11, s32[2,64]{1,0:T(2,128)} %bitcast.13, f32[1,64]{1,0:T(1,128)} %bitcast.15, f32[2,64]{1,0:T(2,128)} %bitcast.14, bf16[32,512]{1,0:T(8,128)(2,1)} %latent.1, ...), custom_call_target="tpu_custom_call" | custom-call | tf_op jit(solution)/shard_map/both_halves/pallas_call | solution.py:1012
  62.5 0.8 %hand_over.1 = (bf16[32,2048]{1,0:T(8,128)(2,1)}, bf16[64,2048]{1,0:T(8,128)(2,1)}) custom-call(bf16[32,2048]{1,0:T(8,128)(2,1)S(1)} %get-tuple-element.4.mixed_in, bf16[64,2048]{1,0:T(8,128)(2,1)S(1)} %get-tuple-element.5.moe_in), custom_call_target="tpu_custom_call" | custom-call | tf_op jit(solution)/shard_map/hand_over/pallas_call | solution.py:1072

commit v4 on v3

--- a/solution.py
+++ b/solution.py
@@ -254,14 +254,14 @@
     heads,
     capacity,
     depth_z,
-    tokens,
-    moe_gain,
-    routes,
-    group_prob,
-    expert_prob,
-    latent,
-    rope_key,
-    latent_gain,
+    tokens_hbm,
+    moe_gain_hbm,
+    routes_hbm,
+    group_prob_hbm,
+    expert_prob_hbm,
+    latent_hbm,
+    rope_key_hbm,
+    latent_gain_hbm,
     query_hbm,
     key_up_hbm,
     value_up_hbm,
@@ -290,6 +290,14 @@
     query_big,
     heads_own,
     heads_all,
+    tokens,
+    moe_gain,
+    routes,
+    group_prob,
+    expert_prob,
+    latent,
+    rope_key,
+    latent_gain,
     query,
     key_up,
     value_up,
@@ -350,7 +358,21 @@
         pltpu.make_async_copy(value_up_hbm, value_up, load_sem.at[5]),
         pltpu.make_async_copy(out_proj_hbm, out_proj, load_sem.at[6]),
     ]
-    for load in loads:
+    small = (
+        (routes_hbm, routes),
+        (expert_prob_hbm, expert_prob),
+        (group_prob_hbm, group_prob),
+        (tokens_hbm, tokens),
+        (moe_gain_hbm, moe_gain),
+        (latent_hbm, latent),
+        (rope_key_hbm, rope_key),
+        (latent_gain_hbm, latent_gain),
+    )
+    early = [
+        pltpu.make_async_copy(src, dst, load_sem.at[7 + number])
+        for number, (src, dst) in enumerate(small)
+    ]
+    for load in early + loads:
         load.start()
 
     def remote(src, dst, sent, got, device):
@@ -480,6 +502,8 @@
             heads_own.at[peer], heads_all.at[slot], (17, number), (17, number), {"tp": peer}
         )
 
+    for load in early:
+        load.wait()
     first_route = routes[0:1, :]
     second_route = routes[1:2, :]
     lane_expert = lax.broadcasted_iota(jnp.int32, (experts, row_count), 0)
@@ -807,25 +831,25 @@
             lat_y(1, 1 - me_y).wait_recv()
             raise_lat(me_z)
 
+        @pl.when(turn >= 4)
+        def _():
+            reduce_pair(turn - 4)
+
+        @pl.when(turn >= 2)
+        def _():
+            compute(turn - 2)
+
+        @pl.when(turn >= 1)
+        def _():
+            relay(turn - 1)
+
+        @pl.when(turn == 2)
+        def _():
+            spread_query()
+
         @pl.when(turn == 6)
         def _():
             take_lat(1)
-
-        @pl.when(turn >= 4)
-        def _():
-            reduce_pair(turn - 4)
-
-        @pl.when(turn >= 2)
-        def _():
-            compute(turn - 2)
-
-        @pl.when(turn >= 1)
-        def _():
-            relay(turn - 1)
-
-        @pl.when(turn == 2)
-        def _():
-            spread_query()
 
         return carry
 
@@ -834,30 +858,39 @@
     pass_y(depth_z - 1, 1)
     share(7)
     reduce_pair(4)
-    send_far(4)
-    take_lat(2)
     compute(5)
     relay(6)
     reduce_pair(3)
     reduce_pair(5)
     send_far(5)
+    send_far(4)
+    take_lat(2)
     compute(6)
+    reduce_pair(6)
+    relay(7)
     take_lat(3)
     lat_mate(0, tp).start()
     lat_mate(1, tp).start()
-    reduce_pair(6)
-    relay(7)
-    lat_mate(0, mate).wait_recv()
-    lat_mate(1, mate).wait_recv()
-    fill_keys()
     compute(7)
     send_far(3)
-    reduce_far(4)
     reduce_far(5)
     reduce_pair(7)
     send_far(7)
     send_far(6)
+    lat_mate(0, mate).wait_recv()
+    lat_mate(1, mate).wait_recv()
+    fill_keys()
     attend(0, heads // 2)
+    reduce_far(4)
+
+    @pl.when(inner)
+    def _():
+        join(2)
+
+    @pl.when(jnp.logical_not(inner))
+    def _():
+        join_pass()
+
     attend(heads // 2, heads)
     for number, peer in enumerate(peers):
         head_copy(number, peer, tp).start()
@@ -866,15 +899,6 @@
     send_far(0)
     heads_all[tp] = heads_own[tp]
     reduce_far(3)
-
-    @pl.when(inner)
-    def _():
-        join(2)
-
-    @pl.when(jnp.logical_not(inner))
-    def _():
-        join_pass()
-
     reduce_far(7)
     reduce_far(6)
 
@@ -1015,7 +1039,7 @@
             pltpu.VMEM((own_rows, out_proj.shape[1]), bf16),
             pltpu.VMEM((row_count, width), bf16),
         ),
-        in_specs=[vmem] * 8 + [anywhere] * 7,
+        in_specs=[anywhere] * 15,
         out_specs=(vmem, vmem),
         scratch_shapes=[
             pltpu.VMEM((depth_z, row_count, width), bf16),
@@ -1037,6 +1061,14 @@
             pltpu.VMEM((heads, query_rows, key_width), bf16),
             pltpu.VMEM((n_tp, own_rows, value_up.shape[1]), bf16),
             pltpu.VMEM((n_tp, own_rows, value_up.shape[1]), bf16),
+            pltpu.VMEM(tokens.shape, bf16),
+            pltpu.VMEM((1, width), jnp.float32),
+            pltpu.VMEM((routes.shape[1], row_count), jnp.int32),
+            pltpu.VMEM((1, row_count), jnp.float32),
+            pltpu.VMEM((routes.shape[1], row_count), jnp.float32),
+            pltpu.VMEM(latent.shape, bf16),
+            pltpu.VMEM(rope_key.shape, bf16),
+            pltpu.VMEM((1, latent_width), jnp.float32),
             pltpu.VMEM(query.shape, bf16),
             pltpu.VMEM(key_up.shape, bf16),
             pltpu.VMEM(value_up.shape, bf16),
@@ -1044,7 +1076,7 @@
             pltpu.VMEM(w_gate.shape[1:], bf16),
             pltpu.VMEM(w_up.shape[1:], bf16),
             pltpu.VMEM(w_down.shape[1:], bf16),
-            pltpu.SemaphoreType.DMA((7,)),
+            pltpu.SemaphoreType.DMA((15,)),
             pltpu.SemaphoreType.DMA((sum(send_kinds(depth_z)),)),
             pltpu.SemaphoreType.DMA((sum(recv_kinds(depth_z)),)),
         ],

time: 63.7 us -> 62 us (0.973)
  Pallas kernels: 62.6 us -> 60.4 us
    pallas_call x1, Pallas kernels: 61.8 us -> 59.7 us  [fused_body(): pl.pallas_call(functools.partial(both_halves, heads, capacity, depth_z),...]
where the time goes in v4:
time: 62 us; the launch traced here: 61.1 us
  Pallas kernels  60.4 us (97%)
  between operations  0.64 us (1%)
    pallas_call x1, Pallas kernels, fused_body(): pl.pallas_call(functools.partial(both_halves, heads, capacity, depth_z),...  59.7 us

profile of v4, /device:TPU:0, one launch (start us, length us, event | category | flops | bytes accessed | tf_op | source)
XLA Modules:
  0.0 61.1 jit_solution(12583824947244132933)
XLA Ops:
  0.6 59.7 %both_halves.1 = (bf16[32,2048]{1,0:T(8,128)(2,1)S(1)}, bf16[64,2048]{1,0:T(8,128)(2,1)S(1)}) custom-call(bf16[64,2048]{1,0:T(8,128)(2,1)} %tokens_hbm.1, f32[1,2048]{1,0:T(1,128)} %bitcast.11, s32[2,64]{1,0:T(2,128)} %bitcast.13, f32[1,64]{1,0:T(1,128)} %bitcast.15, f32[2,64]{1,0:T(2,128)} %bitcast.14, bf16[32,512]{1,0:T(8,128)(2,1)} %latent_hbm.1, ...), custom_call_target="tpu_custom_call" | custom-call | tf_op jit(solution)/shard_map/both_halves/pallas_call | solution.py:1036
  60.3 0.8 %hand_over.1 = (bf16[32,2048]{1,0:T(8,128)(2,1)}, bf16[64,2048]{1,0:T(8,128)(2,1)}) custom-call(bf16[32,2048]{1,0:T(8,128)(2,1)S(1)} %get-tuple-element.4.mixed_in, bf16[64,2048]{1,0:T(8,128)(2,1)S(1)} %get-tuple-element.5.moe_in), custom_call_target="tpu_custom_call" | custom-call | tf_op jit(solution)/shard_map/hand_over/pallas_call | solution.py:1104

commit v5 on v4

--- a/solution.py
+++ b/solution.py
@@ -877,6 +877,7 @@
     reduce_pair(7)
     send_far(7)
     send_far(6)
+    send_far(2)
     lat_mate(0, mate).wait_recv()
     lat_mate(1, mate).wait_recv()
     fill_keys()
@@ -894,7 +895,6 @@
     attend(heads // 2, heads)
     for number, peer in enumerate(peers):
         head_copy(number, peer, tp).start()
-    send_far(2)
     send_far(1)
     send_far(0)
     heads_all[tp] = heads_own[tp]

time: 62 us -> 61.6 us (level)
  no operation moved by 1% of the time
where the time goes in v5:
time: 61.6 us; the launch traced here: 61.1 us
  Pallas kernels  60.4 us (98%)
  between operations  0.64 us (1%)
    pallas_call x1, Pallas kernels, fused_body(): pl.pallas_call(functools.partial(both_halves, heads, capacity, depth_z),...  59.7 us

profile of v5, /device:TPU:0, one launch (start us, length us, event | category | flops | bytes accessed | tf_op | source)
XLA Modules:
  0.0 61.1 jit_solution(9644727092397372628)
XLA Ops:
  0.6 59.7 %both_halves.1 = (bf16[32,2048]{1,0:T(8,128)(2,1)S(1)}, bf16[64,2048]{1,0:T(8,128)(2,1)S(1)}) custom-call(bf16[64,2048]{1,0:T(8,128)(2,1)} %tokens_hbm.1, f32[1,2048]{1,0:T(1,128)} %bitcast.11, s32[2,64]{1,0:T(2,128)} %bitcast.13, f32[1,64]{1,0:T(1,128)} %bitcast.15, f32[2,64]{1,0:T(2,128)} %bitcast.14, bf16[32,512]{1,0:T(8,128)(2,1)} %latent_hbm.1, ...), custom_call_target="tpu_custom_call" | custom-call | tf_op jit(solution)/shard_map/both_halves/pallas_call | solution.py:1036
  60.3 0.8 %hand_over.1 = (bf16[32,2048]{1,0:T(8,128)(2,1)}, bf16[64,2048]{1,0:T(8,128)(2,1)}) custom-call(bf16[32,2048]{1,0:T(8,128)(2,1)S(1)} %get-tuple-element.4.mixed_in, bf16[64,2048]{1,0:T(8,128)(2,1)S(1)} %get-tuple-element.5.moe_in), custom_call_target="tpu_custom_call" | custom-call | tf_op jit(solution)/shard_map/hand_over/pallas_call | solution.py:1104
